TPU v7x, 128 devices: a whole 4x4x4 slice. The times are simulated.
128 devices in a mesh: ep: 16 (over z, x), tp: 8 (over y, core).
Axes of the slice: x: 4, y: 4, z: 4, core: 2. Of those that a mesh axis runs over, the one named last changes fastest.
Arguments:
- mix_tokens: bfloat16 [32768, 2048], P(('ep', 'tp')), may hold values from -40 to 40
- mix_gain: float32 [2048], replicated, may hold values from 0.1 to 1.9
- query_weight: bfloat16 [2048, 1024], replicated, may hold values from -0.125 to 0.125
- key_weight: bfloat16 [2048, 256], replicated, may hold values from -0.125 to 0.125
- value_weight: bfloat16 [2048, 256], replicated, may hold values from -0.125 to 0.125
- query_gain: float32 [64], replicated, may hold values from 0.5 to 40
- key_gain: float32 [64], replicated, may hold values from 0.1 to 1.9
- sink_logits: float32 [16], replicated, may hold values from 2 to 6
- out_weight: bfloat16 [1024, 2048], replicated, may hold values from -0.1875 to 0.1875
- moe_tokens: bfloat16 [16384, 2048], P(('ep', 'tp')), may hold values from -40 to 40
- moe_gain: float32 [2048], replicated, may hold values from 0.1 to 1.9
- routes: int32 [16384, 2], P(('ep', 'tp')), may hold values from 0 to 15, all different within a row; in each aligned block of 128 rows (0 to 127, 128 to 255, ...) at most 18 rows name the same one
- route_logits: float32 [16384, 2], P(('ep', 'tp')), may hold values from -6 to 6
- gate_weight: bfloat16 [16, 2048, 7168], P('ep', None, 'tp'), may hold values from -0.125 to 0.125
- up_weight: bfloat16 [16, 2048, 7168], P('ep', None, 'tp'), may hold values from -0.125 to 0.125
- down_weight: bfloat16 [16, 7168, 2048], P('ep', 'tp'), may hold values from -0.0625 to 0.0625
Outputs:
- mix_out: bfloat16 [32768, 2048], P(('ep', 'tp'))
- moe_out: bfloat16 [16384, 2048], P(('ep', 'tp'))
Inputs may be any that keep to these rules, and one draw needn't show every extreme that they name: `routes`: each row names 2 different experts. Of the rows of one device no expert is named more than 18 times, and in every draw some device names some expert exactly 18 times.
All inputs are finite; a program needn't handle non-finite values.
Results may differ from a plain program's by a relative error of at most 0.015.
The roundings to bfloat16 on the way count: a program that leaves them out, or rounds other values in their place, can miss the bound.
Values may be sent and summed in bfloat16 or wider, within the bound.
No kernel may reach another device: no remote copies, remote signals or barrier semaphores. Data moves between devices by JAX's collectives and lax.ppermute only.
A program may use at most 128 MiB of HBM per device.

v0:
```python
import functools

import jax
import jax.numpy as jnp
from jax import lax
from jax.experimental import pallas as pl
from jax.experimental.pallas import tpu as pltpu
from jax.sharding import PartitionSpec as P

WINDOW = 128
CORES = 2
TILE = 512


epsilon = 1e-06


def passed_along(block, axis, distance):
    devices = range(lax.axis_size(axis))
    route = [(i - distance, i) for i in devices if i - distance in devices]
    return lax.ppermute(block, axis, route)


def outward(block, distance):
    size = lax.axis_size("tp")
    route = [(i, (i + CORES * distance * (1 - 2 * (i % CORES))) % size) for i in range(size)]
    return lax.ppermute(block, "tp", route)


def core_swap(block):
    route = [(i, i ^ 1) for i in range(lax.axis_size("tp"))]
    return lax.ppermute(block, "tp", route)


def rms_scale(values, gain_vec):
    values = values.astype(jnp.float32)
    return (
        values * lax.rsqrt(jnp.mean(values * values, axis=-1, keepdims=True) + epsilon) * gain_vec
    )


def route_slots(routes, experts, capacity):
    flat_ids = routes.reshape(-1)
    onehot = (flat_ids[:, None] == jnp.arange(experts, dtype=jnp.int32)[None, :]).astype(jnp.int32)
    before = jnp.cumsum(onehot, axis=0) - onehot
    slot_ids = jnp.sum(before * onehot, axis=1)
    return (flat_ids * capacity + slot_ids).reshape(routes.shape)


def window_attention(queries, key_ext, value_ext, sink_logits, first_pos):
    row_count = queries.shape[0]
    window_rows = key_ext.shape[0] - row_count
    blocks = row_count // window_rows
    kv_heads = key_ext.shape[1]
    group_size = queries.shape[1] // kv_heads
    head_dim = queries.shape[2]
    query_blk = queries.reshape(blocks, window_rows, kv_heads, group_size, head_dim)

    def pair_up(source):
        lower = source[:row_count].reshape(blocks, window_rows, kv_heads, head_dim)
        upper = source[window_rows:].reshape(blocks, window_rows, kv_heads, head_dim)
        return jnp.concatenate([lower, upper], axis=1)

    key_blk = pair_up(key_ext)
    value_blk = pair_up(value_ext)
    scores = jnp.einsum(
        "bqkgd,bskd->bkgqs", query_blk, key_blk, preferred_element_type=jnp.float32
    ) * head_dim ** (-0.5)
    query_pos = jnp.arange(window_rows, dtype=jnp.int32)[:, None] + window_rows
    key_pos = jnp.arange(2 * window_rows, dtype=jnp.int32)[None, :]
    pos_gap = query_pos - key_pos
    block_start = first_pos + jnp.arange(blocks, dtype=jnp.int32) * window_rows - window_rows
    key_global = block_start[:, None] + jnp.arange(2 * window_rows, dtype=jnp.int32)[None, :]
    visible = ((pos_gap >= 0) & (pos_gap <= window_rows))[None] & (key_global >= 0)[:, None, :]
    scores = jnp.where(visible[:, None, None], scores, -jnp.inf)
    sink_col = sink_logits.reshape(kv_heads, group_size)[None, :, :, None, None]
    row_top = jnp.maximum(jnp.max(scores, axis=-1, keepdims=True), sink_col)
    weights = jnp.exp(scores - row_top)
    denom_sum = jnp.sum(weights, axis=-1, keepdims=True) + jnp.exp(sink_col - row_top)
    attn_prob = (weights / denom_sum).astype(jnp.bfloat16)
    mixed_out = jnp.einsum(
        "bkgqs,bskd->bqkgd", attn_prob, value_blk, preferred_element_type=jnp.float32
    )
    return mixed_out.astype(jnp.bfloat16).reshape(row_count, -1)


def attention(
    mix_tokens,
    mix_gain,
    query_weight,
    key_weight,
    value_weight,
    query_gain,
    key_gain,
    sink_logits,
    out_weight,
):
    row_count = mix_tokens.shape[0]
    head_count = sink_logits.shape[0]
    head_dim = query_gain.shape[0]
    kv_heads = key_weight.shape[1] // head_dim
    normed = rms_scale(mix_tokens, mix_gain).astype(jnp.bfloat16)
    key_rows = jnp.dot(normed, key_weight, preferred_element_type=jnp.float32)
    key_rows = rms_scale(key_rows.reshape(row_count, kv_heads, head_dim), key_gain).astype(
        jnp.bfloat16
    )
    values = jnp.dot(normed, value_weight, preferred_element_type=jnp.float32).astype(
        jnp.bfloat16
    )
    values = values.reshape(row_count, kv_heads, head_dim)
    edge = jnp.concatenate([key_rows[row_count - WINDOW :], values[row_count - WINDOW :]], axis=1)
    rim = passed_along(edge, ("ep", "tp"), 1)
    rim_keys, rim_values = rim[:, :kv_heads], rim[:, kv_heads:]
    queries = jnp.dot(normed, query_weight, preferred_element_type=jnp.float32)
    queries = rms_scale(queries.reshape(row_count, head_count, head_dim), query_gain).astype(
        jnp.bfloat16
    )
    key_ext = jnp.concatenate([rim_keys, key_rows], axis=0)
    value_ext = jnp.concatenate([rim_values, values], axis=0)
    first_pos = lax.axis_index(("ep", "tp")) * row_count
    attended = window_attention(queries, key_ext, value_ext, sink_logits, first_pos)
    return jnp.dot(attended, out_weight, preferred_element_type=jnp.float32).astype(
        jnp.bfloat16
    )


def expert_kernel(count, *refs):
    rows = refs[:count]
    gate_ref, up_ref, down_ref = refs[count : count + 3]
    outs = refs[count + 3 : 2 * count + 3]
    stacked, hidden = refs[2 * count + 3 :]
    inner = gate_ref.shape[1]
    for k in range(count):
        stacked[k] = rows[k][...]

    @pl.loop(0, count)
    def _(k):
        block = stacked[k]
        for low in range(0, inner, TILE):
            cut = slice(low, min(low + TILE, inner))
            gate_act = jnp.dot(block, gate_ref[:, cut], preferred_element_type=jnp.float32)
            up_act = jnp.dot(block, up_ref[:, cut], preferred_element_type=jnp.float32)
            hidden[k, :, cut] = (gate_act * jax.nn.sigmoid(gate_act) * up_act).astype(
                jnp.bfloat16
            )

    @pl.loop(0, down_ref.shape[1] // TILE)
    def _(index):
        cut = pl.ds(pl.multiple_of(index * TILE, TILE), TILE)
        for k in range(count):
            outs[k][:, cut] = jnp.dot(
                hidden[k], down_ref[:, cut], preferred_element_type=jnp.float32
            ).astype(jnp.bfloat16)


def expert_partial(blocks, gate_mat, up_mat, down_mat):
    count = len(blocks)
    rows, width = blocks[0].shape
    inner = gate_mat.shape[1]
    near = pl.BlockSpec(memory_space=pltpu.VMEM)
    return pl.pallas_call(
        functools.partial(expert_kernel, count),
        out_shape=[jax.ShapeDtypeStruct((rows, width), jnp.bfloat16)] * count,
        in_specs=[near] * (count + 3),
        out_specs=[near] * count,
        scratch_shapes=[
            pltpu.VMEM((count, rows, width), jnp.bfloat16),
            pltpu.VMEM((count, rows, inner), jnp.bfloat16),
        ],
        compiler_params=pltpu.CompilerParams(vmem_limit_bytes=24 << 20),
        cost_estimate=pl.CostEstimate(
            flops=6 * count * rows * width * inner,
            transcendentals=count * rows * inner,
            bytes_accessed=2 * (3 * width * inner + 2 * count * rows * width),
        ),
    )(*blocks, gate_mat, up_mat, down_mat)


def added(*parts):
    return sum(part.astype(jnp.float32) for part in parts).astype(jnp.bfloat16)


def exchange(rows, experts):
    count, width = rows.shape
    lanes = 128
    view = rows.reshape(experts, count * width // (experts * lanes), lanes)
    view = lax.all_to_all(view, "ep", split_axis=0, concat_axis=0, tiled=True)
    return view.reshape(count, width)


def body(
    mix_tokens,
    mix_gain,
    query_weight,
    key_weight,
    value_weight,
    query_gain,
    key_gain,
    sink_logits,
    out_weight,
    moe_tokens,
    moe_gain,
    routes,
    route_logits,
    gate_weight,
    up_weight,
    down_weight,
):
    mix_out = attention(
        mix_tokens,
        mix_gain,
        query_weight,
        key_weight,
        value_weight,
        query_gain,
        key_gain,
        sink_logits,
        out_weight,
    )
    moe_rows = moe_tokens.shape[0]
    experts = lax.axis_size("ep")
    capacity = (9 * moe_rows * routes.shape[1] + 8 * experts - 1) // (8 * experts)
    moe_normed = rms_scale(moe_tokens, moe_gain).astype(jnp.bfloat16)
    targets = route_slots(routes, experts, capacity)
    slot_ids = jnp.arange(experts * capacity, dtype=jnp.int32)
    pick_rows = jnp.sum(
        (targets[None, :, :] == slot_ids[:, None, None]).astype(jnp.bfloat16), axis=2
    )
    packed = jnp.dot(pick_rows, moe_normed, preferred_element_type=jnp.float32).astype(jnp.bfloat16)
    own = exchange(packed, experts)

    def run(blocks):
        return expert_partial(blocks, gate_weight[0], up_weight[0], down_weight[0])

    near_a = outward(own, 1)
    own_b = core_swap(own)
    near_b = outward(own_b, 1)
    far_a = outward(near_a, 1)
    across_b = core_swap(near_a)
    across_a = core_swap(near_b)
    far_b = core_swap(far_a)

    own_part_a, own_part_b = run([own, own_b])
    near_part_a, across_part_b = run([near_a, across_b])
    near_part_b, across_part_a = run([near_b, across_a])
    far_part_a, far_part_b = run([far_a, far_b])

    back_a = added(near_part_a, core_swap(across_part_b))
    back_b = added(near_part_b, core_swap(across_part_a))
    far_sum = added(far_part_a, core_swap(far_part_b))
    home_b = outward(back_b, -1)
    passing = outward(far_sum, -1)
    home_a = outward(added(back_a, passing), -1)
    crossing = core_swap(added(own_part_b, home_b))
    total = added(own_part_a, home_a, crossing)
    results = exchange(total, experts)

    gate_probs = jax.nn.softmax(route_logits, axis=-1).astype(jnp.bfloat16)
    combine = jnp.where(
        targets[:, :, None] == slot_ids[None, None, :],
        gate_probs[:, :, None],
        jnp.zeros((), jnp.bfloat16),
    )
    combine = jnp.sum(combine, axis=1)
    moe_out = jnp.dot(combine, results, preferred_element_type=jnp.float32).astype(jnp.bfloat16)
    return (mix_out, moe_out)


def solution(mesh):
    placed = (
        P(("ep", "tp"), None),
        P(),
        P(),
        P(),
        P(),
        P(),
        P(),
        P(),
        P(),
        P(("ep", "tp"), None),
        P(),
        P(("ep", "tp"), None),
        P(("ep", "tp"), None),
        P("ep", None, "tp"),
        P("ep", None, "tp"),
        P("ep", "tp", None),
    )

    return jax.shard_map(
        body,
        mesh=mesh,
        in_specs=placed,
        out_specs=(P(("ep", "tp"), None), P(("ep", "tp"), None)),
        check_vma=False,
    )
```

profile of v0, /device:TPU:1, one launch (start us, length us, event | category | flops | bytes accessed | tf_op | source)
XLA Modules:
  0.0 221.3 jit_solution(11513074456536431181)
XLA Ops:
  0.6 0.9 copy.65
  1.8 0.6 reduce-window.6
  2.9 0.7 multiply_add_fusion
  4.2 1.2 fusion.8
  5.5 1.6 convolution_convert_fusion
  7.1 1.4 reshape.204
  8.5 8.4 %all-to-all-start = ((bf16[16,288,128]{2,1,0:T(8,128)(2,1)}), bf16[16,288,128]{2,1,0:T(8,128)(2,1)S(1)}, u32[]{:S(2)}, u32[]{:S(2)}) async-start(bf16[16,288,128]{2,1,0:T(8,128)(2,1)} %reshape.204), calls=%async_computation | async-start | bytes 2359296 | tf_op jit(solution)/shard_map/all_to_all | solution.py:187
  17.2 17.1 %all-to-all-done = bf16[16,288,128]{2,1,0:T(8,128)(2,1)S(1)} async-done(((bf16[16,288,128]{2,1,0:T(8,128)(2,1)}), bf16[16,288,128]{2,1,0:T(8,128)(2,1)S(1)}, u32[]{:S(2)}, u32[]{:S(2)}) %all-to-all-start) | async-done | bytes 1179680 | tf_op jit(solution)/shard_map/all_to_all | solution.py:187
  34.9 2.8 %collective-permute-start.2 = (bf16[288,2048]{1,0:T(8,128)(2,1)S(1)}, bf16[288,2048]{1,0:T(8,128)(2,1)}, u32[]{:S(2)}, u32[]{:S(2)}) collective-permute-start(bf16[288,2048]{1,0:T(8,128)(2,1)S(1)} %reshape.205.refs_0_), channel_id=1, source_target_pairs={{0,2},{1,7},{2,4},{3,1},{4,6},{5,3},{6,0},{7,5},{8,10},{9,15},{10,... | collective-permute-start | bytes 3538952 | tf_op jit(solution)/shard_map/ppermute | solution.py:27
  37.8 1.9 multiply_reduce_fusion
  39.7 0.6 add_rsqrt_fusion.1
  40.3 1.6 collective-permute-start.1
  42.0 0.7 convolution_convert_fusion.3
  42.8 0.6 copy-done.17
  43.4 0.7 pad_maximum_fusion.2
  44.0 3.1 %collective-permute-start = (bf16[128,8,64]{0,2,1:T(8,128)(2,1)}, bf16[128,8,64]{0,2,1:T(8,128)(2,1)}, u32[]{:S(2)}, u32[]{:S(2)}) collective-permute-start(bf16[128,8,64]{0,2,1:T(8,128)(2,1)} %pad_maximum_fusion.2), channel_id=1, source_target_pairs={{0,1},{1,2},{2,3},{3,4},{4,5},{5,6},{6,7},{7,8},{8,9},{9,10},{10,1... | collective-permute-start | bytes 393224 | tf_op jit(solution)/shard_map/ppermute | solution.py:21
  47.2 3.7 %collective-permute-done.2.refs_0_ = bf16[288,2048]{1,0:T(8,128)(2,1)} collective-permute-done((bf16[288,2048]{1,0:T(8,128)(2,1)S(1)}, bf16[288,2048]{1,0:T(8,128)(2,1)}, u32[]{:S(2)}, u32[]{:S(2)}) %collective-permute-start.2) | collective-permute-done | bytes 1179680 | tf_op jit(solution)/shard_map/ppermute | solution.py:27
  50.9 3.2 %collective-permute-start.5 = (bf16[288,2048]{1,0:T(8,128)(2,1)}, bf16[288,2048]{1,0:T(8,128)(2,1)S(1)}, u32[]{:S(2)}, u32[]{:S(2)}) collective-permute-start(bf16[288,2048]{1,0:T(8,128)(2,1)} %collective-permute-done.2.refs_0_), channel_id=1, source_target_pairs={{0,2},{1,7},{2,4},{3,1},{4,6},{5,3},{6,0},{7,5},{8,10},{9,15},{10,... | collective-permute-start | bytes 3538952 | tf_op jit(solution)/shard_map/ppermute | solution.py:27
  54.1 0.6 fusion.37
  54.7 5.1 %fusion.49 = (f32[256,1024]{1,0:T(8,128)}, f32[256,1024]{1,0:T(8,128)}) fusion(bf16[2048,1024]{1,0:T(8,128)(2,1)} %param.18, bf16[256,2048]{1,0:T(8,128)(2,1)} %param.16, f32[2048]{0:T(1024)} %param.17, f32[256]{0:T(256)S(1)} %add_rsqrt_fusion.2), kind=kOutput, calls=%fused_computation.95 | convolution fusion | flops 1076101120 | bytes 7349248 | tf_op jit(solution)/shard_map/dot_general | solution.py:114
  59.9 2.9 %copy.61 = f32[256,1024]{0,1:T(8,128)} copy(f32[256,1024]{1,0:T(8,128)} %get-tuple-element.22) | data formatting | bytes 2097152 | tf_op jit(solution)/shard_map/mul | solution.py:38
  62.8 1.3 bitcast_reduce_fusion
  64.2 3.4 %collective-permute-done.5.refs_0_ = bf16[288,2048]{1,0:T(8,128)(2,1)S(1)} collective-permute-done((bf16[288,2048]{1,0:T(8,128)(2,1)}, bf16[288,2048]{1,0:T(8,128)(2,1)S(1)}, u32[]{:S(2)}, u32[]{:S(2)}) %collective-permute-start.5) | collective-permute-done | bytes 1179680 | tf_op jit(solution)/shard_map/ppermute | solution.py:27
  67.6 6.7 %collective-permute-start.6 = (bf16[288,2048]{1,0:T(8,128)(2,1)S(1)}, bf16[288,2048]{1,0:T(8,128)(2,1)}, u32[]{:S(2)}, u32[]{:S(2)}) collective-permute-start(bf16[288,2048]{1,0:T(8,128)(2,1)S(1)} %collective-permute-done.5.refs_0_), channel_id=1, source_target_pairs={{0,1},{1,0},{2,3},{3,2},{4,5},{5,4},{6,7},{7,6},{8,9},{9,8},{10,11... | collective-permute-start | bytes 3538952 | tf_op jit(solution)/shard_map/ppermute | solution.py:32
  74.4 0.8 broadcast_and_fusion
  75.1 5.0 %collective-permute-done.10.refs_0_ = bf16[288,2048]{1,0:T(8,128)(2,1)} collective-permute-done((bf16[288,2048]{1,0:T(8,128)(2,1)S(1)}, bf16[288,2048]{1,0:T(8,128)(2,1)}, u32[]{:S(2)}, u32[]{:S(2)}) %collective-permute-start.10) | collective-permute-done | bytes 1179680 | tf_op jit(solution)/shard_map/ppermute | solution.py:27
  80.1 7.0 %collective-permute-start.11 = (bf16[288,2048]{1,0:T(8,128)(2,1)}, bf16[288,2048]{1,0:T(8,128)(2,1)}, u32[]{:S(2)}, u32[]{:S(2)}) collective-permute-start(bf16[288,2048]{1,0:T(8,128)(2,1)} %collective-permute-done.10.refs_0_), channel_id=1, source_target_pairs={{0,1},{1,0},{2,3},{3,2},{4,5},{5,4},{6,7},{7,6},{8,9},{9,8},{10,11... | collective-permute-start | bytes 3538952 | tf_op jit(solution)/shard_map/ppermute | solution.py:32
  87.1 1.3 divide_convert_fusion.6
  88.3 1.8 reshape.200
  90.1 2.5 %copy.60 = f32[256,1024]{0,1:T(8,128)} copy(f32[256,1024]{1,0:T(8,128)} %get-tuple-element.23) | data formatting | bytes 2097152 | tf_op jit(solution)/shard_map/dot_general | solution.py:114
  92.7 2.7 %reshape.201 = f32[2,128,4,4,64]{1,0,4,3,2:T(2,128)} reshape(f32[256,1024]{0,1:T(8,128)} %copy.60) | data formatting | bytes 2097152 | tf_op jit(solution)/shard_map/reshape | solution.py:115
  95.4 1.7 fusion.25
  97.1 2.7 %multiply_convert_fusion = bf16[2,128,4,4,64]{1,0,4,3,2:T(2,128)(2,1)} fusion(f32[2,128,4,4,64]{1,0,4,3,2:T(2,128)} %reshape.201, f32[64]{0:T(128)} %param.21, f32[2,128,4,4]{1,0,3,2:T(2,128)S(1)} %rsqrt.43), kind=kLoop, calls=%fused_computation.29 | loop fusion | flops 786432 | bytes 1589504 | tf_op jit(solution)/shard_map/convert_element_type | solution.py:115
  99.8 2.0 copy-done.2
  101.8 2.0 copy-done.5
  103.9 2.0 copy-done.7
  105.9 11.0 %shard_map.169 = (bf16[288,2048]{1,0:T(8,128)(2,1)S(1)}, bf16[288,2048]{1,0:T(8,128)(2,1)}) custom-call(bf16[288,2048]{1,0:T(8,128)(2,1)S(1)} %collective-permute-done.5.refs_0_, bf16[288,2048]{1,0:T(8,128)(2,1)} %collective-permute-done.6.refs_1_, bf16[2048,896]{1,0:T(8,128)(2,1)S(1)} %bitcast.90, bf16[2048,896]{1,0:T(8,128)(2,1)S(1)} %bitcast.94, ...), custom_call_target="tpu_custom_call" | custom-call | flops 6341787648 | bytes 15728640 | tf_op jit(solution)/shard_map/pallas_call | solution.py:161
  117.4 11.2 %shard_map.170 = (bf16[288,2048]{1,0:T(8,128)(2,1)S(1)}, bf16[288,2048]{1,0:T(8,128)(2,1)}) custom-call(bf16[288,2048]{1,0:T(8,128)(2,1)} %collective-permute-done.10.refs_0_, bf16[288,2048]{1,0:T(8,128)(2,1)} %collective-permute-done.11.refs_1_, bf16[2048,896]{1,0:T(8,128)(2,1)S(1)} %bitcast.91, bf16[2048,896]{1,0:T(8,128)(2,1)S(1)} %bitcast.95, ...), custom_call_target="tpu_custom_call" | custom-call | flops 6341787648 | bytes 15728640 | tf_op jit(solution)/shard_map/pallas_call | solution.py:161
  128.6 0.7 fusion.27
  129.3 1.6 reshape_reshape.3
  130.9 1.6 copy.57
  132.5 2.0 copy-done.4
  134.6 2.0 copy-done.6
  136.6 2.0 copy-done.8
  138.6 10.1 %shard_map.168 = (bf16[288,2048]{1,0:T(8,128)(2,1)S(1)}, bf16[288,2048]{1,0:T(8,128)(2,1)S(1)}) custom-call(bf16[288,2048]{1,0:T(8,128)(2,1)} %collective-permute-done.2.refs_0_, bf16[288,2048]{1,0:T(8,128)(2,1)} %collective-permute-done.3.refs_1_, bf16[2048,896]{1,0:T(8,128)(2,1)S(1)} %bitcast.92, bf16[2048,896]{1,0:T(8,128)(2,1)S(1)} %bitcast.96, ...), custom_call_target="tpu_custom_call" | custom-call | flops 6341787648 | bytes 15728640 | tf_op jit(solution)/shard_map/pallas_call | solution.py:161
  148.8 0.6 collective-permute-start.4
  149.3 1.7 add_convert_fusion.4
  151.2 1.8 add_convert_fusion.2
  153.1 0.9 fusion.48
  154.0 8.5 %shard_map.167 = (bf16[288,2048]{1,0:T(8,128)(2,1)S(1)}, bf16[288,2048]{1,0:T(8,128)(2,1)S(1)}) custom-call(bf16[288,2048]{1,0:T(8,128)(2,1)S(1)} %reshape.205.refs_0_, bf16[288,2048]{1,0:T(8,128)(2,1)S(1)} %copy-done.10, bf16[2048,896]{1,0:T(8,128)(2,1)S(1)} %bitcast.93, bf16[2048,896]{1,0:T(8,128)(2,1)S(1)} %bitcast.97, bf16[896,2048]{1,0:T(8,128)(2,1)S(1)} %bitcast.101), custom_call_target="tpu_custom_call" | custom-call | flops 6341787648 | bytes 15728640 | tf_op jit(solution)/shard_map/pallas_call | solution.py:161
  162.5 4.9 %collective-permute-done.8 = bf16[288,2048]{1,0:T(8,128)(2,1)S(1)} collective-permute-done((bf16[288,2048]{1,0:T(8,128)(2,1)S(1)}, bf16[288,2048]{1,0:T(8,128)(2,1)S(1)}, u32[]{:S(2)}, u32[]{:S(2)}) %collective-permute-start.8) | collective-permute-done | bytes 1179680 | tf_op jit(solution)/shard_map/ppermute | solution.py:27
  167.4 0.7 add_convert_fusion.3
  168.2 11.9 %collective-permute-done.13 = bf16[288,2048]{1,0:T(8,128)(2,1)S(1)} collective-permute-done((bf16[288,2048]{1,0:T(8,128)(2,1)S(1)}, bf16[288,2048]{1,0:T(8,128)(2,1)S(1)}, u32[]{:S(2)}, u32[]{:S(2)}) %collective-permute-start.13) | collective-permute-done | bytes 1179680 | tf_op jit(solution)/shard_map/ppermute | solution.py:27
  181.1 0.8 fusion.1
  182.0 1.0 fusion
  183.0 9.6 %collective-permute-done.9 = bf16[288,2048]{1,0:T(8,128)(2,1)S(1)} collective-permute-done((bf16[288,2048]{1,0:T(8,128)(2,1)S(1)}, bf16[288,2048]{1,0:T(8,128)(2,1)S(1)}, u32[]{:S(2)}, u32[]{:S(2)}) %collective-permute-start.9) | collective-permute-done | bytes 1179680 | tf_op jit(solution)/shard_map/ppermute | solution.py:27
  192.7 0.6 add_convert_fusion
  193.3 1.4 reshape.206
  194.7 3.7 %all-to-all-start.1 = ((bf16[16,288,128]{2,1,0:T(8,128)(2,1)}), bf16[16,288,128]{2,1,0:T(8,128)(2,1)S(1)}, u32[]{:S(2)}, u32[]{:S(2)}) async-start(bf16[16,288,128]{2,1,0:T(8,128)(2,1)} %reshape.206), calls=%async_computation.1 | async-start | bytes 2359296 | tf_op jit(solution)/shard_map/all_to_all | solution.py:187
  198.4 3.5 %fusion.7 = bf16[2,128,4,4,64]{1,4,3,2,0:T(8,128)(2,1)S(1)} fusion(f32[2,4,256,128,4]{3,2,4,1,0:T(8,128)} %copy-done.11, f32[2,4,4,128]{3,2,1,0:T(4,128)S(1)} %exponential_add_fusion, f32[2,4,4,128]{3,2,1,0:T(4,128)S(1)} %broadcast_maximum_fusion, pred[2,128,256]{1,2,0:T(8,128)(4,1)S(1)} %copy-done.21, bf16[2,128,4,64]{1,3,2,0:T(8,128)(2,1)S(1)} %copy-done.23, ...), kind=kOutput, calls=%fused_computation.23 | convolution fusion | flops 140247040 | bytes 5079040 | tf_op jit(solution)/shard_map/bkgqs,bskd->bqkgd/dot_general | solution.py:81
  201.9 0.5 copy.64
  202.5 2.3 %convolution_convert_fusion.1 = bf16[256,2048]{1,0:T(8,128)(2,1)} fusion(bf16[1024,2048]{1,0:T(8,128)(2,1)S(1)} %copy-done.31, bf16[128,8,2,128]{3,2,1,0:T(2,128)(2,1)S(1)} %bitcast.103), kind=kOutput, calls=%fused_computation.8 | convolution fusion | flops 1074266112 | bytes 5767168 | tf_op jit(solution)/shard_map/dot_general | solution.py:122
  204.8 14.7 %all-to-all-done.1 = bf16[16,288,128]{2,1,0:T(8,128)(2,1)S(1)} async-done(((bf16[16,288,128]{2,1,0:T(8,128)(2,1)}), bf16[16,288,128]{2,1,0:T(8,128)(2,1)S(1)}, u32[]{:S(2)}, u32[]{:S(2)}) %all-to-all-start.1) | async-done | bytes 1179680 | tf_op jit(solution)/shard_map/all_to_all | solution.py:187
  220.0 1.3 convolution_convert_fusion.2
  (112 shorter events, 5.3 us)
Async XLA Ops:
  0.6 37.1 %copy-start = (bf16[2048,256]{1,0:T(8,128)(2,1)S(1)}, bf16[2048,256]{1,0:T(8,128)(2,1)}, u32[]{:S(2)}) copy-start(bf16[2048,256]{1,0:T(8,128)(2,1)} %param.19) | copy-start | bytes 3145732
  3.6 0.5 copy-start.24
  7.1 9.8 %copy-start.12 = (bf16[256,2048]{1,0:T(8,128)(2,1)S(1)}, bf16[256,2048]{1,0:T(8,128)(2,1)}, u32[]{:S(2)}) copy-start(bf16[256,2048]{1,0:T(8,128)(2,1)} %param.16) | copy-start | bytes 3145732
  8.5 25.9 %all-to-all-start = ((bf16[16,288,128]{2,1,0:T(8,128)(2,1)}), bf16[16,288,128]{2,1,0:T(8,128)(2,1)S(1)}, u32[]{:S(2)}, u32[]{:S(2)}) async-start(bf16[16,288,128]{2,1,0:T(8,128)(2,1)} %reshape.204), calls=%async_computation | async-start | bytes 2359296 | tf_op jit(solution)/shard_map/all_to_all | solution.py:187
  17.2 20.5 %copy-start.33 = (f32[2048]{0:T(1024)S(1)}, f32[2048]{0:T(1024)}, u32[]{:S(2)}) copy-start(f32[2048]{0:T(1024)} %param.17) | copy-start | bytes 24580
  34.9 7.0 %copy-start.28 = (f32[64]{0:T(128)S(1)}, f32[64]{0:T(128)}, u32[]{:S(2)}) copy-start(f32[64]{0:T(128)} %param.22) | copy-start | bytes 772
  34.9 7.1 %copy-start.13 = (bf16[256,2048]{1,0:T(8,128)(2,1)S(1)}, bf16[256,2048]{1,0:T(8,128)(2,1)}, u32[]{:S(2)}) copy-start(bf16[256,2048]{1,0:T(8,128)(2,1)} %param.16) | copy-start | bytes 3145732
  34.9 7.1 %copy-start.32 = (bf16[2048,256]{1,0:T(8,128)(2,1)S(1)}, bf16[2048,256]{1,0:T(8,128)(2,1)}, u32[]{:S(2)}) copy-start(bf16[2048,256]{1,0:T(8,128)(2,1)} %param.20) | copy-start | bytes 3145732
  34.9 7.1 %copy-start.34 = (f32[2048]{0:T(1024)S(1)}, f32[2048]{0:T(1024)}, u32[]{:S(2)}) copy-start(f32[2048]{0:T(1024)} %param.17) | copy-start | bytes 24580
  34.9 15.9 %collective-permute-start.2 = (bf16[288,2048]{1,0:T(8,128)(2,1)S(1)}, bf16[288,2048]{1,0:T(8,128)(2,1)}, u32[]{:S(2)}, u32[]{:S(2)}) collective-permute-start(bf16[288,2048]{1,0:T(8,128)(2,1)S(1)} %reshape.205.refs_0_), channel_id=1, source_target_pairs={{0,2},{1,7},{2,4},{3,1},{4,6},{5,3},{6,0},{7,5},{8,10},{9,15},{10,... | collective-permute-start | bytes 3538952 | tf_op jit(solution)/shard_map/ppermute | solution.py:27
  39.6 3.1 %copy-start.14 = (f32[256,256]{0,1:T(8,128)}, f32[256,256]{0,1:T(8,128)S(1)}, u32[]{:S(2)}) copy-start(f32[256,256]{0,1:T(8,128)S(1)} %get-tuple-element.25) | copy-start | bytes 786436
  39.7 7.5 %copy-start.26 = (f32[128,2]{0,1:T(2,128)S(1)}, f32[128,2]{0,1:T(2,128)}, u32[]{:S(2)}) copy-start(f32[128,2]{0,1:T(2,128)} %param.28) | copy-start | bytes 3076
  40.3 19.6 %collective-permute-start.1 = (bf16[288,2048]{1,0:T(8,128)(2,1)S(1)}, bf16[288,2048]{1,0:T(8,128)(2,1)S(1)}, u32[]{:S(2)}, u32[]{:S(2)}) collective-permute-start(bf16[288,2048]{1,0:T(8,128)(2,1)S(1)} %reshape.205.refs_0_), channel_id=1, source_target_pairs={{0,1},{1,0},{2,3},{3,2},{4,5},{5,4},{6,7},{7,6},{8,9},{9,8},{10,11... | collective-permute-start | bytes 3538952 | tf_op jit(solution)/shard_map/ppermute | solution.py:32
  42.0 5.2 %copy-start.15 = (bf16[256,4,64]{0,2,1:T(8,128)(2,1)}, bf16[256,4,64]{0,2,1:T(8,128)(2,1)S(1)}, u32[]{:S(2)}) copy-start(bf16[256,4,64]{0,2,1:T(8,128)(2,1)S(1)} %multiply_convert_fusion.1) | copy-start | bytes 393220
  42.7 0.7 copy-start.17
  44.0 109.1 %collective-permute-start = (bf16[128,8,64]{0,2,1:T(8,128)(2,1)}, bf16[128,8,64]{0,2,1:T(8,128)(2,1)}, u32[]{:S(2)}, u32[]{:S(2)}) collective-permute-start(bf16[128,8,64]{0,2,1:T(8,128)(2,1)} %pad_maximum_fusion.2), channel_id=1, source_target_pairs={{0,1},{1,2},{2,3},{3,4},{4,5},{5,6},{6,7},{7,8},{8,9},{9,10},{10,1... | collective-permute-start | bytes 393224 | tf_op jit(solution)/shard_map/ppermute | solution.py:21
  47.2 12.7 %copy-start.27 = (f32[128]{0:T(128)}, f32[128]{0:T(128)S(1)}, u32[]{:S(2)}) copy-start(f32[128]{0:T(128)S(1)} %reduce_max.19) | copy-start | bytes 1540
  50.9 16.7 %collective-permute-start.5 = (bf16[288,2048]{1,0:T(8,128)(2,1)}, bf16[288,2048]{1,0:T(8,128)(2,1)S(1)}, u32[]{:S(2)}, u32[]{:S(2)}) collective-permute-start(bf16[288,2048]{1,0:T(8,128)(2,1)} %collective-permute-done.2.refs_0_), channel_id=1, source_target_pairs={{0,2},{1,7},{2,4},{3,1},{4,6},{5,3},{6,0},{7,5},{8,10},{9,15},{10,... | collective-permute-start | bytes 3538952 | tf_op jit(solution)/shard_map/ppermute | solution.py:27
  59.8 32.8 %copy-start.9 = (bf16[288,2048]{1,0:T(8,128)(2,1)}, bf16[288,2048]{1,0:T(8,128)(2,1)S(1)}, u32[]{:S(2)}) copy-start(bf16[288,2048]{1,0:T(8,128)(2,1)S(1)} %collective-permute-done.1.refs_1_) | copy-start | bytes 3538948
  59.8 20.3 %collective-permute-start.10 = (bf16[288,2048]{1,0:T(8,128)(2,1)S(1)}, bf16[288,2048]{1,0:T(8,128)(2,1)}, u32[]{:S(2)}, u32[]{:S(2)}) collective-permute-start(bf16[288,2048]{1,0:T(8,128)(2,1)S(1)} %collective-permute-done.1.refs_1_), channel_id=1, source_target_pairs={{0,2},{1,7},{2,4},{3,1},{4,6},{5,3},{6,0},{7,5},{8,10},{9,15},{10,... | collective-permute-start | bytes 3538952 | tf_op jit(solution)/shard_map/ppermute | solution.py:27
  67.6 32.2 %collective-permute-start.6 = (bf16[288,2048]{1,0:T(8,128)(2,1)S(1)}, bf16[288,2048]{1,0:T(8,128)(2,1)}, u32[]{:S(2)}, u32[]{:S(2)}) collective-permute-start(bf16[288,2048]{1,0:T(8,128)(2,1)S(1)} %collective-permute-done.5.refs_0_), channel_id=1, source_target_pairs={{0,1},{1,0},{2,3},{3,2},{4,5},{5,4},{6,7},{7,6},{8,9},{9,8},{10,11... | collective-permute-start | bytes 3538952 | tf_op jit(solution)/shard_map/ppermute | solution.py:32
  80.1 37.2 %collective-permute-start.11 = (bf16[288,2048]{1,0:T(8,128)(2,1)}, bf16[288,2048]{1,0:T(8,128)(2,1)}, u32[]{:S(2)}, u32[]{:S(2)}) collective-permute-start(bf16[288,2048]{1,0:T(8,128)(2,1)} %collective-permute-done.10.refs_0_), channel_id=1, source_target_pairs={{0,1},{1,0},{2,3},{3,2},{4,5},{5,4},{6,7},{7,6},{8,9},{9,8},{10,11... | collective-permute-start | bytes 3538952 | tf_op jit(solution)/shard_map/ppermute | solution.py:32
  99.8 32.8 %collective-permute-start.3 = (bf16[288,2048]{1,0:T(8,128)(2,1)}, bf16[288,2048]{1,0:T(8,128)(2,1)}, u32[]{:S(2)}, u32[]{:S(2)}) collective-permute-start(bf16[288,2048]{1,0:T(8,128)(2,1)} %collective-permute-done.2.refs_0_), channel_id=1, source_target_pairs={{0,1},{1,0},{2,3},{3,2},{4,5},{5,4},{6,7},{7,6},{8,9},{9,8},{10,11... | collective-permute-start | bytes 3538952 | tf_op jit(solution)/shard_map/ppermute | solution.py:32
  99.8 2.0 copy-start.2
  101.8 2.0 copy-start.5
  103.9 2.0 copy-start.7
  105.9 11.5 %copy-start.3 = (bf16[1,2048,896]{2,1,0:T(8,128)(2,1)S(1)}, bf16[1,2048,896]{2,1,0:T(8,128)(2,1)}, u32[]{:S(2)}) copy-start(bf16[1,2048,896]{2,1,0:T(8,128)(2,1)} %param.29) | copy-start | bytes 11010052
  116.8 11.8 %copy-start.25 = (s32[128,2]{0,1:T(2,128)S(1)}, s32[128,2]{0,1:T(2,128)}, u32[]{:S(2)}) copy-start(s32[128,2]{0,1:T(2,128)} %copy-done.24) | copy-start | bytes 3076
  116.8 11.8 %copy-start.29 = (bf16[128,2]{0,1:T(2,128)(2,1)S(1)}, bf16[128,2]{0,1:T(2,128)(2,1)}, u32[]{:S(2)}) copy-start(bf16[128,2]{0,1:T(2,128)(2,1)} %divide_convert_fusion.6) | copy-start | bytes 1540
  116.9 14.0 %copy-start.30 = (f32[16]{0:T(128)S(1)}, f32[16]{0:T(128)}, u32[]{:S(2)}) copy-start(f32[16]{0:T(128)} %param.23) | copy-start | bytes 196
  116.9 32.5 %collective-permute-start.7 = (bf16[288,2048]{1,0:T(8,128)(2,1)}, bf16[288,2048]{1,0:T(8,128)(2,1)}, u32[]{:S(2)}, u32[]{:S(2)}) collective-permute-start(bf16[288,2048]{1,0:T(8,128)(2,1)} %get-tuple-element.14), channel_id=1, source_target_pairs={{0,1},{1,0},{2,3},{3,2},{4,5},{5,4},{6,7},{7,6},{8,9},{9,8},{10,11... | collective-permute-start | bytes 3538952 | tf_op jit(solution)/shard_map/ppermute | solution.py:32
  128.6 22.6 %collective-permute-start.12 = (bf16[288,2048]{1,0:T(8,128)(2,1)}, bf16[288,2048]{1,0:T(8,128)(2,1)}, u32[]{:S(2)}, u32[]{:S(2)}) collective-permute-start(bf16[288,2048]{1,0:T(8,128)(2,1)} %get-tuple-element.17), channel_id=1, source_target_pairs={{0,1},{1,0},{2,3},{3,2},{4,5},{5,4},{6,7},{7,6},{8,9},{9,8},{10,11... | collective-permute-start | bytes 3538952 | tf_op jit(solution)/shard_map/ppermute | solution.py:32
  132.5 2.0 copy-start.4
  134.6 2.0 copy-start.6
  136.6 2.0 copy-start.8
  148.8 13.7 %collective-permute-start.4 = (bf16[288,2048]{1,0:T(8,128)(2,1)S(1)}, bf16[288,2048]{1,0:T(8,128)(2,1)S(1)}, u32[]{:S(2)}, u32[]{:S(2)}) collective-permute-start(bf16[288,2048]{1,0:T(8,128)(2,1)S(1)} %get-tuple-element.12), channel_id=1, source_target_pairs={{0,1},{1,0},{2,3},{3,2},{4,5},{5,4},{6,7},{7,6},{8,9},{9,8},{10,11... | collective-permute-start | bytes 3538952 | tf_op jit(solution)/shard_map/ppermute | solution.py:32
  151.0 2.9 %copy-start.10 = (bf16[288,2048]{1,0:T(8,128)(2,1)S(1)}, bf16[288,2048]{1,0:T(8,128)(2,1)}, u32[]{:S(2)}) copy-start(bf16[288,2048]{1,0:T(8,128)(2,1)} %copy-done.9) | copy-start | bytes 3538948
  151.1 16.3 %collective-permute-start.8 = (bf16[288,2048]{1,0:T(8,128)(2,1)S(1)}, bf16[288,2048]{1,0:T(8,128)(2,1)S(1)}, u32[]{:S(2)}, u32[]{:S(2)}) collective-permute-start(bf16[288,2048]{1,0:T(8,128)(2,1)S(1)} %add_convert_fusion.4), channel_id=1, source_target_pairs={{0,6},{1,3},{2,0},{3,5},{4,2},{5,7},{6,4},{7,1},{8,14},{9,11},{10,... | collective-permute-start | bytes 3538952 | tf_op jit(solution)/shard_map/ppermute | solution.py:27
  152.9 27.1 %collective-permute-start.13 = (bf16[288,2048]{1,0:T(8,128)(2,1)S(1)}, bf16[288,2048]{1,0:T(8,128)(2,1)S(1)}, u32[]{:S(2)}, u32[]{:S(2)}) collective-permute-start(bf16[288,2048]{1,0:T(8,128)(2,1)S(1)} %add_convert_fusion.2), channel_id=1, source_target_pairs={{0,6},{1,3},{2,0},{3,5},{4,2},{5,7},{6,4},{7,1},{8,14},{9,11},{10,... | collective-permute-start | bytes 3538952 | tf_op jit(solution)/shard_map/ppermute | solution.py:27
  168.1 12.8 %copy-start.16 = (bf16[256,4,64]{0,2,1:T(8,128)(2,1)S(1)}, bf16[256,4,64]{0,2,1:T(8,128)(2,1)}, u32[]{:S(2)}) copy-start(bf16[256,4,64]{0,2,1:T(8,128)(2,1)} %copy-done.15) | copy-start | bytes 393220
  168.1 12.8 %copy-start.18 = (bf16[256,256]{0,1:T(8,128)(2,1)S(1)}, bf16[256,256]{0,1:T(8,128)(2,1)}, u32[]{:S(2)}) copy-start(bf16[256,256]{0,1:T(8,128)(2,1)} %copy-done.17) | copy-start | bytes 393220
  168.1 24.6 %collective-permute-start.9 = (bf16[288,2048]{1,0:T(8,128)(2,1)S(1)}, bf16[288,2048]{1,0:T(8,128)(2,1)S(1)}, u32[]{:S(2)}, u32[]{:S(2)}) collective-permute-start(bf16[288,2048]{1,0:T(8,128)(2,1)S(1)} %add_convert_fusion.3), channel_id=1, source_target_pairs={{0,6},{1,3},{2,0},{3,5},{4,2},{5,7},{6,4},{7,1},{8,14},{9,11},{10,... | collective-permute-start | bytes 3538952 | tf_op jit(solution)/shard_map/ppermute | solution.py:27
  180.0 1.0 copy-start.19
  180.0 1.0 copy-start.21
  180.0 1.1 copy-start.22
  180.5 12.2 %collective-permute-start.14 = (bf16[288,2048]{1,0:T(8,128)(2,1)S(1)}, bf16[288,2048]{1,0:T(8,128)(2,1)S(1)}, u32[]{:S(2)}, u32[]{:S(2)}) collective-permute-start(bf16[288,2048]{1,0:T(8,128)(2,1)S(1)} %add_convert_fusion.1), channel_id=1, source_target_pairs={{0,1},{1,0},{2,3},{3,2},{4,5},{5,4},{6,7},{7,6},{8,9},{9,8},{10,11... | collective-permute-start | bytes 3538952 | tf_op jit(solution)/shard_map/ppermute | solution.py:32
  181.9 10.8 %copy-start.11 = (f32[2,4,256,128,4]{3,2,4,1,0:T(8,128)}, f32[2,4,256,128,4]{3,2,4,1,0:T(8,128)S(1)}, u32[]{:S(2)}) copy-start(f32[2,4,256,128,4]{3,2,4,1,0:T(8,128)S(1)} %get-tuple-element.27) | copy-start | bytes 12582916
  193.3 5.1 %copy-start.23 = (bf16[2,128,4,64]{1,3,2,0:T(8,128)(2,1)S(1)}, bf16[2,128,4,64]{1,3,2,0:T(8,128)(2,1)}, u32[]{:S(2)}) copy-start(bf16[2,128,4,64]{1,3,2,0:T(8,128)(2,1)} %copy.57) | copy-start | bytes 393220
  194.7 24.8 %all-to-all-start.1 = ((bf16[16,288,128]{2,1,0:T(8,128)(2,1)}), bf16[16,288,128]{2,1,0:T(8,128)(2,1)S(1)}, u32[]{:S(2)}, u32[]{:S(2)}) async-start(bf16[16,288,128]{2,1,0:T(8,128)(2,1)} %reshape.206), calls=%async_computation.1 | async-start | bytes 2359296 | tf_op jit(solution)/shard_map/all_to_all | solution.py:187
  198.4 4.1 %copy-start.31 = (bf16[1024,2048]{1,0:T(8,128)(2,1)S(1)}, bf16[1024,2048]{1,0:T(8,128)(2,1)}, u32[]{:S(2)}) copy-start(bf16[1024,2048]{1,0:T(8,128)(2,1)} %param.24) | copy-start | bytes 12582916
  202.5 18.8 %copy-start.1 = (bf16[2048,256]{1,0:T(8,128)(2,1)S(1)}, bf16[2048,256]{1,0:T(8,128)(2,1)}, u32[]{:S(2)}) copy-start(bf16[2048,256]{1,0:T(8,128)(2,1)} %param.19) | copy-start | bytes 3145732
  204.8 15.3 %copy-start.20 = (bf16[128,288]{0,1:T(8,128)(2,1)S(1)}, bf16[128,288]{0,1:T(8,128)(2,1)}, u32[]{:S(2)}) copy-start(bf16[128,288]{0,1:T(8,128)(2,1)} %fusion.27) | copy-start | bytes 221188
where the time goes:
time: 222 us; the launch traced here: 221 us
  waiting for transfers between devices  70.3 us (32%)
  Pallas kernels  40.8 us (18%)
  starting transfers between devices  38.3 us (17%)
  local copies, waits for them, and re-layouts  33.8 us (15%)
  other arithmetic  19.8 us (9%)
  matrix products  17.1 us (8%)
    pallas_call x4, Pallas kernels, expert_partial(): pl.pallas_call(functools.partial(expert_kernel, count), out_shape=[jax.Sh...  40.8 us
    ppermute x6, waiting for transfers between devices, outward(): return lax.ppermute(block, 'tp', route)  38.5 us
    all_to_all x2, waiting for transfers between devices, exchange(): view = lax.all_to_all(view, 'ep', split_axis=0, concat_axis=0, tiled=True)  31.9 us
    ppermute x8, starting transfers between devices, core_swap(): return lax.ppermute(block, 'tp', route)  16.7 us
    unnamed x71, local copies, waits for them, and re-layouts  14.6 us
    all_to_all x2, starting transfers between devices, exchange(): view = lax.all_to_all(view, 'ep', split_axis=0, concat_axis=0, tiled=True)  12.1 us
    ppermute x6, starting transfers between devices, outward(): return lax.ppermute(block, 'tp', route)  6.39 us
    convert_element_type x5, other arithmetic, added(): sum((part.astype(jnp.float32) for part in parts)).astype(jnp.bfloat16)  5.21 us
  transfers between devices with their start and end apart: 17, of which 8 were waited for; matrix products, arithmetic and copies ran while one was open for 21% of the time, Pallas kernels for 18%

commit v1 on v0

--- a/solution.py
+++ b/solution.py
@@ -39,12 +39,74 @@
     )
 
 
-def route_slots(routes, experts, capacity):
-    flat_ids = routes.reshape(-1)
-    onehot = (flat_ids[:, None] == jnp.arange(experts, dtype=jnp.int32)[None, :]).astype(jnp.int32)
-    before = jnp.cumsum(onehot, axis=0) - onehot
-    slot_ids = jnp.sum(before * onehot, axis=1)
-    return (flat_ids * capacity + slot_ids).reshape(routes.shape)
+def pack_kernel(capacity, *refs):
+    sources, (packed_ref, targets_ref) = refs[:3], refs[3:5]
+    tokens_ref, gain_ref, routes_ref = held = refs[5:8]
+    copies = [
+        pltpu.make_async_copy(source, place, refs[8].at[n])
+        for n, (source, place) in enumerate(zip(sources, held))
+    ]
+    for copy in copies:
+        copy.start()
+    for copy in copies:
+        copy.wait()
+    experts = packed_ref.shape[0] // capacity
+    count = tokens_ref.shape[0]
+    values = tokens_ref[...].astype(jnp.float32)
+    scale = lax.rsqrt(jnp.mean(values * values, axis=-1, keepdims=True) + epsilon)
+    normed = (values * scale * gain_ref[...]).astype(jnp.bfloat16)
+    expert_ids = lax.broadcasted_iota(jnp.int32, (experts, count), 0)
+    named_by = [expert_ids == routes_ref[k : k + 1, :] for k in range(routes_ref.shape[0])]
+    routed = functools.reduce(jnp.logical_or, named_by).astype(jnp.float32)
+    earlier = lax.broadcasted_iota(jnp.int32, (count, count), 0) < lax.broadcasted_iota(
+        jnp.int32, (count, count), 1
+    )
+    slots = jnp.dot(
+        routed.astype(jnp.bfloat16),
+        earlier.astype(jnp.float32).astype(jnp.bfloat16),
+        preferred_element_type=jnp.float32,
+    )
+    for k, mask in enumerate(named_by):
+        places = slots + (expert_ids * capacity).astype(jnp.float32)
+        targets_ref[k : k + 1, :] = jnp.sum(
+            jnp.where(mask, places, 0.0), axis=0, keepdims=True
+        ).astype(jnp.int32)
+    rows = packed_ref.shape[0]
+    lows = lax.broadcasted_iota(jnp.int32, (rows, experts), 1) * capacity
+    row_ids = lax.broadcasted_iota(jnp.int32, (rows, experts), 0)
+    owner = (row_ids >= lows) & (row_ids < lows + capacity)
+    spread = jnp.dot(
+        owner.astype(jnp.float32).astype(jnp.bfloat16),
+        (routed * (slots + 1.0)).astype(jnp.bfloat16),
+        preferred_element_type=jnp.float32,
+    )
+    wanted = jnp.sum(jnp.where(owner, row_ids - lows + 1, 0).astype(jnp.float32), axis=1)
+    pick = (spread == wanted[:, None]).astype(jnp.float32).astype(jnp.bfloat16)
+    packed_ref[...] = jnp.dot(pick, normed, preferred_element_type=jnp.float32).astype(
+        jnp.bfloat16
+    )
+
+
+def packed_rows(tokens, gain_vec, routes, experts, capacity):
+    near = pl.BlockSpec(memory_space=pltpu.VMEM)
+    width = tokens.shape[1]
+    packed, targets = pl.pallas_call(
+        functools.partial(pack_kernel, capacity),
+        out_shape=[
+            jax.ShapeDtypeStruct((experts * capacity, width), jnp.bfloat16),
+            jax.ShapeDtypeStruct(routes.shape[::-1], jnp.int32),
+        ],
+        in_specs=[pl.BlockSpec(memory_space=pl.ANY)] * 3,
+        out_specs=[near] * 2,
+        scratch_shapes=[
+            pltpu.VMEM(tokens.shape, tokens.dtype),
+            pltpu.VMEM((1, width), gain_vec.dtype),
+            pltpu.VMEM(routes.shape[::-1], routes.dtype),
+            pltpu.SemaphoreType.DMA((3,)),
+        ],
+        compiler_params=pltpu.CompilerParams(vmem_limit_bytes=16 << 20),
+    )(tokens, gain_vec.reshape(1, width), routes.T)
+    return packed, targets.T
 
 
 def window_attention(queries, key_ext, value_ext, sink_logits, first_pos):
@@ -176,8 +238,22 @@
     )(*blocks, gate_mat, up_mat, down_mat)
 
 
+def add_kernel(*refs):
+    total = refs[0][...].astype(jnp.float32)
+    for ref in refs[1:-1]:
+        total = total + ref[...].astype(jnp.float32)
+    refs[-1][...] = total.astype(refs[-1].dtype)
+
+
 def added(*parts):
-    return sum(part.astype(jnp.float32) for part in parts).astype(jnp.bfloat16)
+    near = pl.BlockSpec(memory_space=pltpu.VMEM)
+    return pl.pallas_call(
+        add_kernel,
+        out_shape=jax.ShapeDtypeStruct(parts[0].shape, parts[0].dtype),
+        in_specs=[near] * len(parts),
+        out_specs=near,
+        compiler_params=pltpu.CompilerParams(vmem_limit_bytes=12 << 20),
+    )(*parts)
 
 
 def exchange(rows, experts):
@@ -220,13 +296,8 @@
     moe_rows = moe_tokens.shape[0]
     experts = lax.axis_size("ep")
     capacity = (9 * moe_rows * routes.shape[1] + 8 * experts - 1) // (8 * experts)
-    moe_normed = rms_scale(moe_tokens, moe_gain).astype(jnp.bfloat16)
-    targets = route_slots(routes, experts, capacity)
+    packed, targets = packed_rows(moe_tokens, moe_gain, routes, experts, capacity)
     slot_ids = jnp.arange(experts * capacity, dtype=jnp.int32)
-    pick_rows = jnp.sum(
-        (targets[None, :, :] == slot_ids[:, None, None]).astype(jnp.bfloat16), axis=2
-    )
-    packed = jnp.dot(pick_rows, moe_normed, preferred_element_type=jnp.float32).astype(jnp.bfloat16)
     own = exchange(packed, experts)
 
     def run(blocks):
@@ -240,10 +311,13 @@
     across_a = core_swap(near_b)
     far_b = core_swap(far_a)
 
-    own_part_a, own_part_b = run([own, own_b])
+    (own_part_a,) = run([own])
+    (own_part_b,) = run([own_b])
     near_part_a, across_part_b = run([near_a, across_b])
-    near_part_b, across_part_a = run([near_b, across_a])
-    far_part_a, far_part_b = run([far_a, far_b])
+    (near_part_b,) = run([near_b])
+    (across_part_a,) = run([across_a])
+    (far_part_a,) = run([far_a])
+    (far_part_b,) = run([far_b])
 
     back_a = added(near_part_a, core_swap(across_part_b))
     back_b = added(near_part_b, core_swap(across_part_a))

time: 222 us -> 212 us (0.955)
  waiting for transfers between devices: 70.3 us -> 43.5 us
  blocking collectives: 0 us -> 25.8 us
  Pallas kernels: 40.8 us -> 52.2 us
  other arithmetic: 19.8 us -> 10.1 us
  starting transfers between devices: 38.3 us -> 30.9 us
  matrix products: 17.1 us -> 13.2 us
    all_to_all x0 -> x1, blocking collectives: none -> 25.8 us  [exchange(): view = lax.all_to_all(view, 'ep', split_axis=0, concat_axis=0, tiled=True)]
    all_to_all x2 -> x1, waiting for transfers between devices: 31.9 us -> 14.7 us  [exchange(): view = lax.all_to_all(view, 'ep', split_axis=0, concat_axis=0, tiled=True)]
    ppermute x6, waiting for transfers between devices: 38.5 us -> 28.7 us  [outward(): return lax.ppermute(block, 'tp', route)]
    pallas_call x0 -> x7, Pallas kernels: none -> 8.93 us  [the longest x6 8.14 us: added(): pl.pallas_call(add_kernel, out_shape=jax.ShapeDtypeStruct(parts[0].shape,...]
    all_to_all x2 -> x1, starting transfers between devices: 12.1 us -> 3.7 us  [exchange(): view = lax.all_to_all(view, 'ep', split_axis=0, concat_axis=0, tiled=True)]
    convert_element_type x6 -> x0, other arithmetic: 5.22 us -> none  [the longest x5 5.21 us: added(): sum((part.astype(jnp.float32) for part in parts)).astype(jnp.bfloat16)]
    unnamed x71 -> x78, local copies, waits for them, and re-layouts: 14.6 us -> 18 us
    pallas_call x4 -> x7, Pallas kernels: 40.8 us -> 43.3 us  [expert_partial(): pl.pallas_call(functools.partial(expert_kernel, count), out_shape=[jax.Sh...]
  transfers between devices with their start and end apart: 17 -> 16, of which waited for: 8 -> 7; matrix products, arithmetic and copies ran while one was open for 21% -> 16% of each run, Pallas kernels for 18% -> 24%
where the time goes in v1:
time: 212 us; the launch traced here: 211 us
  Pallas kernels  52.2 us (25%)
  waiting for transfers between devices  43.5 us (21%)
  local copies, waits for them, and re-layouts  34.1 us (16%)
  starting transfers between devices  30.9 us (15%)
  blocking collectives  25.8 us (12%)
  matrix products  13.2 us (6%)
  other arithmetic  10.1 us (5%)
    pallas_call x7, Pallas kernels, expert_partial(): pl.pallas_call(functools.partial(expert_kernel, count), out_shape=[jax.Sh...  43.3 us
    ppermute x6, waiting for transfers between devices, outward(): return lax.ppermute(block, 'tp', route)  28.7 us
    all_to_all x1, blocking collectives, exchange(): view = lax.all_to_all(view, 'ep', split_axis=0, concat_axis=0, tiled=True)  25.8 us
    unnamed x78, local copies, waits for them, and re-layouts  18 us
    ppermute x8, starting transfers between devices, core_swap(): return lax.ppermute(block, 'tp', route)  14.8 us
    all_to_all x1, waiting for transfers between devices, exchange(): view = lax.all_to_all(view, 'ep', split_axis=0, concat_axis=0, tiled=True)  14.7 us
    pallas_call x6, Pallas kernels, added(): pl.pallas_call(add_kernel, out_shape=jax.ShapeDtypeStruct(parts[0].shape,...  8.14 us
    ppermute x6, starting transfers between devices, outward(): return lax.ppermute(block, 'tp', route)  7.26 us
  transfers between devices with their start and end apart: 16, of which 7 were waited for; matrix products, arithmetic and copies ran while one was open for 16% of the time, Pallas kernels for 24%

profile of v1, /device:TPU:1, one launch (start us, length us, event | category | flops | bytes accessed | tf_op | source)
XLA Modules:
  0.0 211.1 jit_solution(821063386704015979)
XLA Ops:
  0.7 1.1 copy-done.13
  1.8 0.7 copy-done.14
  2.5 0.7 copy-done.15
  3.2 0.8 shard_map.167
  4.6 25.8 %all_to_all.10 = bf16[16,288,128]{2,1,0:T(8,128)(2,1)} all-to-all(bf16[16,288,128]{2,1,0:T(8,128)(2,1)S(1)} %reshape.169), channel_id=1, replica_groups=mesh['ep'=16,'tp'=8] {'ep'}, dimensions={0} | all-to-all | bytes 2359296 | tf_op jit(solution)/shard_map/all_to_all | solution.py:263
  30.4 2.3 %reshape.170.refs_0_ = bf16[288,2048]{1,0:T(8,128)(2,1)S(1)} reshape(bf16[16,288,128]{2,1,0:T(8,128)(2,1)} %all_to_all.10) | data formatting | bytes 2359296 | tf_op jit(solution)/shard_map/reshape | solution.py:264
  32.7 2.8 %collective-permute-start.1 = (bf16[288,2048]{1,0:T(8,128)(2,1)S(1)}, bf16[288,2048]{1,0:T(8,128)(2,1)}, u32[]{:S(2)}, u32[]{:S(2)}) collective-permute-start(bf16[288,2048]{1,0:T(8,128)(2,1)S(1)} %reshape.170.refs_0_), channel_id=1, source_target_pairs={{0,2},{1,7},{2,4},{3,1},{4,6},{5,3},{6,0},{7,5},{8,10},{9,15},{10,... | collective-permute-start | bytes 3538952 | tf_op jit(solution)/shard_map/ppermute | solution.py:27
  35.8 1.0 collective-permute-start.9
  36.8 2.0 multiply_reduce_fusion
  38.9 9.8 %collective-permute-done.1.refs_0_ = bf16[288,2048]{1,0:T(8,128)(2,1)} collective-permute-done((bf16[288,2048]{1,0:T(8,128)(2,1)S(1)}, bf16[288,2048]{1,0:T(8,128)(2,1)}, u32[]{:S(2)}, u32[]{:S(2)}) %collective-permute-start.1) | collective-permute-done | bytes 1179680 | tf_op jit(solution)/shard_map/ppermute | solution.py:27
  48.7 3.2 %collective-permute-start.4 = (bf16[288,2048]{1,0:T(8,128)(2,1)}, bf16[288,2048]{1,0:T(8,128)(2,1)}, u32[]{:S(2)}, u32[]{:S(2)}) collective-permute-start(bf16[288,2048]{1,0:T(8,128)(2,1)} %collective-permute-done.1.refs_0_), channel_id=1, source_target_pairs={{0,2},{1,7},{2,4},{3,1},{4,6},{5,3},{6,0},{7,5},{8,10},{9,15},{10,... | collective-permute-start | bytes 3538952 | tf_op jit(solution)/shard_map/ppermute | solution.py:27
  52.1 0.7 convolution_convert_fusion.2
  52.9 0.7 pad_maximum_fusion.2
  53.6 5.2 %collective-permute-start = (bf16[128,8,64]{0,2,1:T(8,128)(2,1)}, bf16[128,8,64]{0,2,1:T(8,128)(2,1)}, u32[]{:S(2)}, u32[]{:S(2)}) collective-permute-start(bf16[128,8,64]{0,2,1:T(8,128)(2,1)} %pad_maximum_fusion.2), channel_id=1, source_target_pairs={{0,1},{1,2},{2,3},{3,4},{4,5},{5,6},{6,7},{7,8},{8,9},{9,10},{10,1... | collective-permute-start | bytes 393224 | tf_op jit(solution)/shard_map/ppermute | solution.py:21
  58.7 2.7 %fusion.37 = (f32[256,1024]{1,0:T(8,128)}, f32[256,1024]{1,0:T(8,128)}) fusion(bf16[2048,1024]{1,0:T(8,128)(2,1)S(1)} %copy-done.35, bf16[256,2048]{1,0:T(8,128)(2,1)S(1)} %copy-done.18, f32[2048]{0:T(1024)S(1)} %copy-done.38, f32[256]{0:T(256)S(1)} %add_rsqrt_fusion.2), kind=kOutput, calls=%fused_computation.67 | convolution fusion | flops 1076101120 | bytes 7349248 | tf_op jit(solution)/shard_map/dot_general | solution.py:176
  61.4 1.6 copy.40
  63.6 1.8 collective-permute-done.4.refs_0_
  65.4 6.1 %collective-permute-start.5 = (bf16[288,2048]{1,0:T(8,128)(2,1)}, bf16[288,2048]{1,0:T(8,128)(2,1)}, u32[]{:S(2)}, u32[]{:S(2)}) collective-permute-start(bf16[288,2048]{1,0:T(8,128)(2,1)} %collective-permute-done.4.refs_0_), channel_id=1, source_target_pairs={{0,1},{1,0},{2,3},{3,2},{4,5},{5,4},{6,7},{7,6},{8,9},{9,8},{10,11... | collective-permute-start | bytes 3538952 | tf_op jit(solution)/shard_map/ppermute | solution.py:32
  72.2 5.7 %collective-permute-done.10.refs_0_ = bf16[288,2048]{1,0:T(8,128)(2,1)} collective-permute-done((bf16[288,2048]{1,0:T(8,128)(2,1)S(1)}, bf16[288,2048]{1,0:T(8,128)(2,1)}, u32[]{:S(2)}, u32[]{:S(2)}) %collective-permute-start.10) | collective-permute-done | bytes 1179680 | tf_op jit(solution)/shard_map/ppermute | solution.py:27
  77.9 6.2 %collective-permute-start.11 = (bf16[288,2048]{1,0:T(8,128)(2,1)}, bf16[288,2048]{1,0:T(8,128)(2,1)}, u32[]{:S(2)}, u32[]{:S(2)}) collective-permute-start(bf16[288,2048]{1,0:T(8,128)(2,1)} %collective-permute-done.10.refs_0_), channel_id=1, source_target_pairs={{0,1},{1,0},{2,3},{3,2},{4,5},{5,4},{6,7},{7,6},{8,9},{9,8},{10,11... | collective-permute-start | bytes 3538952 | tf_op jit(solution)/shard_map/ppermute | solution.py:32
  84.7 1.8 reshape.165
  86.5 2.5 %copy.39 = f32[256,1024]{0,1:T(8,128)} copy(f32[256,1024]{1,0:T(8,128)} %get-tuple-element.15) | data formatting | bytes 2097152 | tf_op jit(solution)/shard_map/dot_general | solution.py:176
  89.0 1.7 reshape.166
  90.8 1.3 rsqrt.35
  92.1 0.7 fusion.24
  92.9 1.7 fusion.18
  94.6 2.2 %multiply_convert_fusion = bf16[2,128,4,4,64]{1,0,4,3,2:T(2,128)(2,1)} fusion(f32[2,128,4,4,64]{1,0,4,3,2:T(2,128)S(1)} %reshape.166, f32[64]{0:T(128)} %param.21, f32[2,128,4,4]{1,0,3,2:T(2,128)} %rsqrt.35), kind=kLoop, calls=%fused_computation.17 | loop fusion | flops 786432 | bytes 1589504 | tf_op jit(solution)/shard_map/convert_element_type | solution.py:177
  96.8 2.0 copy-done.2
  98.9 2.0 copy-done.5
  100.9 2.0 copy-done.8
  102.9 5.8 %shard_map.172 = bf16[288,2048]{1,0:T(8,128)(2,1)S(1)} custom-call(bf16[288,2048]{1,0:T(8,128)(2,1)} %collective-permute-done.5.refs_0_, bf16[2048,896]{1,0:T(8,128)(2,1)S(1)} %bitcast.73, bf16[2048,896]{1,0:T(8,128)(2,1)S(1)} %bitcast.80, bf16[896,2048]{1,0:T(8,128)(2,1)S(1)} %bitcast.87), custom_call_target="tpu_custom_call" | custom-call | flops 3170893824 | bytes 13369344 | tf_op jit(solution)/shard_map/pallas_call | solution.py:223
  108.8 0.8 collective-permute-start.6
  109.5 5.8 %shard_map.177 = bf16[288,2048]{1,0:T(8,128)(2,1)S(1)} custom-call(bf16[288,2048]{1,0:T(8,128)(2,1)} %collective-permute-done.11.refs_0_, bf16[2048,896]{1,0:T(8,128)(2,1)S(1)} %bitcast.74, bf16[2048,896]{1,0:T(8,128)(2,1)S(1)} %bitcast.81, bf16[896,2048]{1,0:T(8,128)(2,1)S(1)} %bitcast.88), custom_call_target="tpu_custom_call" | custom-call | flops 3170893824 | bytes 13369344 | tf_op jit(solution)/shard_map/pallas_call | solution.py:223
  115.5 10.8 %shard_map.169 = (bf16[288,2048]{1,0:T(8,128)(2,1)S(1)}, bf16[288,2048]{1,0:T(8,128)(2,1)}) custom-call(bf16[288,2048]{1,0:T(8,128)(2,1)} %collective-permute-done.1.refs_0_, bf16[288,2048]{1,0:T(8,128)(2,1)S(1)} %collective-permute-done.2.refs_1_, bf16[2048,896]{1,0:T(8,128)(2,1)S(1)} %bitcast.75, bf16[2048,896]{1,0:T(8,128)(2,1)S(1)} %bitcast.82, ...), custom_call_target="tpu_custom_call" | custom-call | flops 6341787648 | bytes 15728640 | tf_op jit(solution)/shard_map/pallas_call | solution.py:223
  126.3 1.0 copy-done.11
  127.8 5.8 %shard_map.171.refs_0_ = bf16[288,2048]{1,0:T(8,128)(2,1)S(1)} custom-call(bf16[288,2048]{1,0:T(8,128)(2,1)} %collective-permute-done.4.refs_0_, bf16[2048,896]{1,0:T(8,128)(2,1)S(1)} %bitcast.76, bf16[2048,896]{1,0:T(8,128)(2,1)S(1)} %bitcast.83, bf16[896,2048]{1,0:T(8,128)(2,1)S(1)} %bitcast.90), custom_call_target="tpu_custom_call" | custom-call | flops 3170893824 | bytes 13369344 | tf_op jit(solution)/shard_map/pallas_call | solution.py:223
  133.7 5.8 %shard_map.176.refs_0_ = bf16[288,2048]{1,0:T(8,128)(2,1)S(1)} custom-call(bf16[288,2048]{1,0:T(8,128)(2,1)} %collective-permute-done.10.refs_0_, bf16[2048,896]{1,0:T(8,128)(2,1)S(1)} %bitcast.77, bf16[2048,896]{1,0:T(8,128)(2,1)S(1)} %bitcast.84, bf16[896,2048]{1,0:T(8,128)(2,1)S(1)} %bitcast.91), custom_call_target="tpu_custom_call" | custom-call | flops 3170893824 | bytes 13369344 | tf_op jit(solution)/shard_map/pallas_call | solution.py:223
  139.5 1.3 shard_map.173
  140.9 1.3 shard_map.178
  142.7 0.7 copy.36
  143.3 0.7 fusion.19
  144.0 0.9 fusion.36
  145.0 2.0 copy-done.3
  147.0 2.0 copy-done.6
  149.1 2.0 copy-done.9
  151.1 4.6 %shard_map.175.refs_0_ = bf16[288,2048]{1,0:T(8,128)(2,1)S(1)} custom-call(bf16[288,2048]{1,0:T(8,128)(2,1)S(1)} %collective-permute-done.9.refs_0_, bf16[2048,896]{1,0:T(8,128)(2,1)S(1)} %bitcast.78, bf16[2048,896]{1,0:T(8,128)(2,1)S(1)} %bitcast.85, bf16[896,2048]{1,0:T(8,128)(2,1)S(1)} %bitcast.92), custom_call_target="tpu_custom_call" | custom-call | flops 3170893824 | bytes 13369344 | tf_op jit(solution)/shard_map/pallas_call | solution.py:223
  155.7 1.7 shard_map.170.refs_0_
  157.4 1.7 shard_map.174
  159.1 1.0 collective-permute-start.8
  160.1 10.0 %collective-permute-done.13.refs_1_ = bf16[288,2048]{1,0:T(8,128)(2,1)} collective-permute-done((bf16[288,2048]{1,0:T(8,128)(2,1)}, bf16[288,2048]{1,0:T(8,128)(2,1)}, u32[]{:S(2)}, u32[]{:S(2)}) %collective-permute-start.13) | collective-permute-done | bytes 1179680 | tf_op jit(solution)/shard_map/ppermute | solution.py:27
  170.1 1.8 shard_map.179
  172.0 0.8 fusion.1
  172.9 0.9 fusion
  173.9 1.1 copy-done.16
  175.0 0.7 exponential_add_fusion
  175.6 1.0 copy-done.4
  176.7 4.6 %shard_map.168.refs_0_ = bf16[288,2048]{1,0:T(8,128)(2,1)S(1)} custom-call(bf16[288,2048]{1,0:T(8,128)(2,1)S(1)} %reshape.170.refs_0_, bf16[2048,896]{1,0:T(8,128)(2,1)S(1)} %bitcast.79, bf16[2048,896]{1,0:T(8,128)(2,1)S(1)} %bitcast.86, bf16[896,2048]{1,0:T(8,128)(2,1)S(1)} %bitcast.93), custom_call_target="tpu_custom_call" | custom-call | flops 3170893824 | bytes 13369344 | tf_op jit(solution)/shard_map/pallas_call | solution.py:223
  181.2 1.4 collective-permute-done.8.refs_1_
  183.1 1.4 reshape.171
  184.5 3.7 %all-to-all-start.1 = ((bf16[16,288,128]{2,1,0:T(8,128)(2,1)}), bf16[16,288,128]{2,1,0:T(8,128)(2,1)S(1)}, u32[]{:S(2)}, u32[]{:S(2)}) async-start(bf16[16,288,128]{2,1,0:T(8,128)(2,1)} %reshape.171), calls=%async_computation.1 | async-start | bytes 2359296 | tf_op jit(solution)/shard_map/all_to_all | solution.py:263
  188.3 3.5 %fusion.7 = bf16[2,128,4,4,64]{1,4,3,2,0:T(8,128)(2,1)S(1)} fusion(f32[2,4,256,128,4]{3,2,4,1,0:T(8,128)} %copy-done.16, f32[2,4,4,128]{3,2,1,0:T(4,128)S(1)} %copy-done.30, f32[2,4,4,128]{3,2,1,0:T(4,128)S(1)} %copy-done.29, pred[2,128,256]{1,2,0:T(8,128)(4,1)S(1)} %copy-done.25, bf16[2,128,4,64]{1,3,2,0:T(8,128)(2,1)S(1)} %copy-done.27, ...), kind=kOutput, calls=%fused_computation.14 | convolution fusion | flops 140247040 | bytes 5079040 | tf_op jit(solution)/shard_map/bkgqs,bskd->bqkgd/dot_general | solution.py:143
  192.4 2.2 %convolution_convert_fusion = bf16[256,2048]{1,0:T(8,128)(2,1)} fusion(bf16[1024,2048]{1,0:T(8,128)(2,1)S(1)} %copy-done.36, bf16[128,8,2,128]{3,2,1,0:T(2,128)(2,1)S(1)} %bitcast.98), kind=kOutput, calls=%fused_computation.7 | convolution fusion | flops 1074266112 | bytes 5767168 | tf_op jit(solution)/shard_map/dot_general | solution.py:184
  194.6 14.7 %all-to-all-done.1 = bf16[16,288,128]{2,1,0:T(8,128)(2,1)S(1)} async-done(((bf16[16,288,128]{2,1,0:T(8,128)(2,1)}), bf16[16,288,128]{2,1,0:T(8,128)(2,1)S(1)}, u32[]{:S(2)}, u32[]{:S(2)}) %all-to-all-start.1) | async-done | bytes 1179680 | tf_op jit(solution)/shard_map/all_to_all | solution.py:263
  209.8 1.3 convolution_convert_fusion.1
  (108 shorter events, 6.1 us)
Async XLA Ops:
  0.6 36.2 %copy-start = (bf16[2048,256]{1,0:T(8,128)(2,1)S(1)}, bf16[2048,256]{1,0:T(8,128)(2,1)}, u32[]{:S(2)}) copy-start(bf16[2048,256]{1,0:T(8,128)(2,1)} %param.19) | copy-start | bytes 3145732
  0.6 1.1 copy-start.13
  1.8 0.7 copy-start.14
  2.5 0.7 copy-start.15
  30.3 5.2 %copy-start.17 = (bf16[256,2048]{1,0:T(8,128)(2,1)S(1)}, bf16[256,2048]{1,0:T(8,128)(2,1)}, u32[]{:S(2)}) copy-start(bf16[256,2048]{1,0:T(8,128)(2,1)} %param.16) | copy-start | bytes 3145732
  30.3 6.5 %copy-start.38 = (f32[2048]{0:T(1024)S(1)}, f32[2048]{0:T(1024)}, u32[]{:S(2)}) copy-start(f32[2048]{0:T(1024)} %param.17) | copy-start | bytes 24580
  32.7 19.2 %copy-start.32 = (f32[64]{0:T(128)S(1)}, f32[64]{0:T(128)}, u32[]{:S(2)}) copy-start(f32[64]{0:T(128)} %param.22) | copy-start | bytes 772
  32.7 19.3 %copy-start.18 = (bf16[256,2048]{1,0:T(8,128)(2,1)S(1)}, bf16[256,2048]{1,0:T(8,128)(2,1)}, u32[]{:S(2)}) copy-start(bf16[256,2048]{1,0:T(8,128)(2,1)} %param.16) | copy-start | bytes 3145732
  32.7 19.3 %copy-start.37 = (bf16[2048,256]{1,0:T(8,128)(2,1)S(1)}, bf16[2048,256]{1,0:T(8,128)(2,1)}, u32[]{:S(2)}) copy-start(bf16[2048,256]{1,0:T(8,128)(2,1)} %param.20) | copy-start | bytes 3145732
  32.7 16.0 %collective-permute-start.1 = (bf16[288,2048]{1,0:T(8,128)(2,1)S(1)}, bf16[288,2048]{1,0:T(8,128)(2,1)}, u32[]{:S(2)}, u32[]{:S(2)}) collective-permute-start(bf16[288,2048]{1,0:T(8,128)(2,1)S(1)} %reshape.170.refs_0_), channel_id=1, source_target_pairs={{0,2},{1,7},{2,4},{3,1},{4,6},{5,3},{6,0},{7,5},{8,10},{9,15},{10,... | collective-permute-start | bytes 3538952 | tf_op jit(solution)/shard_map/ppermute | solution.py:27
  35.8 16.9 %collective-permute-start.9 = (bf16[288,2048]{1,0:T(8,128)(2,1)S(1)}, bf16[288,2048]{1,0:T(8,128)(2,1)S(1)}, u32[]{:S(2)}, u32[]{:S(2)}) collective-permute-start(bf16[288,2048]{1,0:T(8,128)(2,1)S(1)} %reshape.170.refs_0_), channel_id=1, source_target_pairs={{0,1},{1,0},{2,3},{3,2},{4,5},{5,4},{6,7},{7,6},{8,9},{9,8},{10,11... | collective-permute-start | bytes 3538952 | tf_op jit(solution)/shard_map/ppermute | solution.py:32
  36.8 21.9 %copy-start.35 = (bf16[2048,1024]{1,0:T(8,128)(2,1)S(1)}, bf16[2048,1024]{1,0:T(8,128)(2,1)}, u32[]{:S(2)}) copy-start(bf16[2048,1024]{1,0:T(8,128)(2,1)} %param.18) | copy-start | bytes 12582916
  38.9 13.9 %copy-start.19 = (f32[256,256]{0,1:T(8,128)}, f32[256,256]{0,1:T(8,128)S(1)}, u32[]{:S(2)}) copy-start(f32[256,256]{0,1:T(8,128)S(1)} %get-tuple-element.17) | copy-start | bytes 786436
  48.7 16.7 %collective-permute-start.4 = (bf16[288,2048]{1,0:T(8,128)(2,1)}, bf16[288,2048]{1,0:T(8,128)(2,1)}, u32[]{:S(2)}, u32[]{:S(2)}) collective-permute-start(bf16[288,2048]{1,0:T(8,128)(2,1)} %collective-permute-done.1.refs_0_), channel_id=1, source_target_pairs={{0,2},{1,7},{2,4},{3,1},{4,6},{5,3},{6,0},{7,5},{8,10},{9,15},{10,... | collective-permute-start | bytes 3538952 | tf_op jit(solution)/shard_map/ppermute | solution.py:27
  52.8 8.6 %copy-start.20 = (bf16[256,256]{0,1:T(8,128)(2,1)}, bf16[256,256]{0,1:T(8,128)(2,1)S(1)}, u32[]{:S(2)}) copy-start(bf16[256,256]{0,1:T(8,128)(2,1)S(1)} %convolution_convert_fusion.2) | copy-start | bytes 393220
  52.8 25.1 %collective-permute-start.10 = (bf16[288,2048]{1,0:T(8,128)(2,1)S(1)}, bf16[288,2048]{1,0:T(8,128)(2,1)}, u32[]{:S(2)}, u32[]{:S(2)}) collective-permute-start(bf16[288,2048]{1,0:T(8,128)(2,1)S(1)} %collective-permute-done.9.refs_0_), channel_id=1, source_target_pairs={{0,2},{1,7},{2,4},{3,1},{4,6},{5,3},{6,0},{7,5},{8,10},{9,15},{10,... | collective-permute-start | bytes 3538952 | tf_op jit(solution)/shard_map/ppermute | solution.py:27
  53.6 90.5 %collective-permute-start = (bf16[128,8,64]{0,2,1:T(8,128)(2,1)}, bf16[128,8,64]{0,2,1:T(8,128)(2,1)}, u32[]{:S(2)}, u32[]{:S(2)}) collective-permute-start(bf16[128,8,64]{0,2,1:T(8,128)(2,1)} %pad_maximum_fusion.2), channel_id=1, source_target_pairs={{0,1},{1,2},{2,3},{3,4},{4,5},{5,6},{6,7},{7,8},{8,9},{9,10},{10,1... | collective-permute-start | bytes 393224 | tf_op jit(solution)/shard_map/ppermute | solution.py:21
  65.4 31.4 %collective-permute-start.5 = (bf16[288,2048]{1,0:T(8,128)(2,1)}, bf16[288,2048]{1,0:T(8,128)(2,1)}, u32[]{:S(2)}, u32[]{:S(2)}) collective-permute-start(bf16[288,2048]{1,0:T(8,128)(2,1)} %collective-permute-done.4.refs_0_), channel_id=1, source_target_pairs={{0,1},{1,0},{2,3},{3,2},{4,5},{5,4},{6,7},{7,6},{8,9},{9,8},{10,11... | collective-permute-start | bytes 3538952 | tf_op jit(solution)/shard_map/ppermute | solution.py:32
  77.9 31.6 %collective-permute-start.11 = (bf16[288,2048]{1,0:T(8,128)(2,1)}, bf16[288,2048]{1,0:T(8,128)(2,1)}, u32[]{:S(2)}, u32[]{:S(2)}) collective-permute-start(bf16[288,2048]{1,0:T(8,128)(2,1)} %collective-permute-done.10.refs_0_), channel_id=1, source_target_pairs={{0,1},{1,0},{2,3},{3,2},{4,5},{5,4},{6,7},{7,6},{8,9},{9,8},{10,11... | collective-permute-start | bytes 3538952 | tf_op jit(solution)/shard_map/ppermute | solution.py:32
  86.5 5.6 %copy-start.31 = (f32[128,2]{0,1:T(2,128)S(1)}, f32[128,2]{0,1:T(2,128)}, u32[]{:S(2)}) copy-start(f32[128,2]{0,1:T(2,128)} %param.28) | copy-start | bytes 3076
  92.8 22.7 %collective-permute-start.2 = (bf16[288,2048]{1,0:T(8,128)(2,1)}, bf16[288,2048]{1,0:T(8,128)(2,1)S(1)}, u32[]{:S(2)}, u32[]{:S(2)}) collective-permute-start(bf16[288,2048]{1,0:T(8,128)(2,1)} %collective-permute-done.1.refs_0_), channel_id=1, source_target_pairs={{0,1},{1,0},{2,3},{3,2},{4,5},{5,4},{6,7},{7,6},{8,9},{9,8},{10,11... | collective-permute-start | bytes 3538952 | tf_op jit(solution)/shard_map/ppermute | solution.py:32
  96.8 2.0 copy-start.2
  98.9 2.0 copy-start.5
  100.9 2.0 copy-start.8
  108.8 30.7 %collective-permute-start.6 = (bf16[288,2048]{1,0:T(8,128)(2,1)S(1)}, bf16[288,2048]{1,0:T(8,128)(2,1)S(1)}, u32[]{:S(2)}, u32[]{:S(2)}) collective-permute-start(bf16[288,2048]{1,0:T(8,128)(2,1)S(1)} %shard_map.172), channel_id=1, source_target_pairs={{0,1},{1,0},{2,3},{3,2},{4,5},{5,4},{6,7},{7,6},{8,9},{9,8},{10,11... | collective-permute-start | bytes 3538952 | tf_op jit(solution)/shard_map/ppermute | solution.py:32
  115.4 25.5 %collective-permute-start.12 = (bf16[288,2048]{1,0:T(8,128)(2,1)S(1)}, bf16[288,2048]{1,0:T(8,128)(2,1)S(1)}, u32[]{:S(2)}, u32[]{:S(2)}) collective-permute-start(bf16[288,2048]{1,0:T(8,128)(2,1)S(1)} %shard_map.177), channel_id=1, source_target_pairs={{0,1},{1,0},{2,3},{3,2},{4,5},{5,4},{6,7},{7,6},{8,9},{9,8},{10,11... | collective-permute-start | bytes 3538952 | tf_op jit(solution)/shard_map/ppermute | solution.py:32
  126.3 1.0 copy-start.11
  127.4 28.3 %collective-permute-start.3 = (bf16[288,2048]{1,0:T(8,128)(2,1)}, bf16[288,2048]{1,0:T(8,128)(2,1)}, u32[]{:S(2)}, u32[]{:S(2)}) collective-permute-start(bf16[288,2048]{1,0:T(8,128)(2,1)} %get-tuple-element.9), channel_id=1, source_target_pairs={{0,1},{1,0},{2,3},{3,2},{4,5},{5,4},{6,7},{7,6},{8,9},{9,8},{10,11... | collective-permute-start | bytes 3538952 | tf_op jit(solution)/shard_map/ppermute | solution.py:32
  140.9 1.5 copy-start.33
  140.9 1.7 copy-start.21
  140.9 1.7 copy-start.34
  140.9 16.6 %collective-permute-start.7 = (bf16[288,2048]{1,0:T(8,128)(2,1)}, bf16[288,2048]{1,0:T(8,128)(2,1)}, u32[]{:S(2)}, u32[]{:S(2)}) collective-permute-start(bf16[288,2048]{1,0:T(8,128)(2,1)} %shard_map.173), channel_id=1, source_target_pairs={{0,6},{1,3},{2,0},{3,5},{4,2},{5,7},{6,4},{7,1},{8,14},{9,11},{10,... | collective-permute-start | bytes 3538952 | tf_op jit(solution)/shard_map/ppermute | solution.py:27
  142.2 27.9 %collective-permute-start.13 = (bf16[288,2048]{1,0:T(8,128)(2,1)}, bf16[288,2048]{1,0:T(8,128)(2,1)}, u32[]{:S(2)}, u32[]{:S(2)}) collective-permute-start(bf16[288,2048]{1,0:T(8,128)(2,1)} %shard_map.178), channel_id=1, source_target_pairs={{0,6},{1,3},{2,0},{3,5},{4,2},{5,7},{6,4},{7,1},{8,14},{9,11},{10,... | collective-permute-start | bytes 3538952 | tf_op jit(solution)/shard_map/ppermute | solution.py:27
  142.5 30.4 %copy-start.24 = (pred[2,128,256]{1,2,0:T(8,128)(4,1)}, pred[2,128,256]{1,2,0:T(8,128)(4,1)S(1)}, u32[]{:S(2)}) copy-start(pred[2,128,256]{1,2,0:T(8,128)(4,1)S(1)} %broadcast_and_fusion) | copy-start | bytes 196612
  145.0 2.0 copy-start.3
  147.0 2.0 copy-start.6
  149.1 2.0 copy-start.9
  151.1 4.6 %copy-start.12 = (bf16[288,2048]{1,0:T(8,128)(2,1)S(1)}, bf16[288,2048]{1,0:T(8,128)(2,1)}, u32[]{:S(2)}) copy-start(bf16[288,2048]{1,0:T(8,128)(2,1)} %copy-done.11) | copy-start | bytes 3538948
  159.1 12.9 %copy-start.22 = (bf16[2,128,4,4,64]{1,0,4,3,2:T(2,128)(2,1)S(1)}, bf16[2,128,4,4,64]{1,0,4,3,2:T(2,128)(2,1)}, u32[]{:S(2)}) copy-start(bf16[2,128,4,4,64]{1,0,4,3,2:T(2,128)(2,1)} %multiply_convert_fusion) | copy-start | bytes 1572868
  159.1 12.9 %copy-start.26 = (bf16[2,128,4,64]{1,3,2,0:T(8,128)(2,1)S(1)}, bf16[2,128,4,64]{1,3,2,0:T(8,128)(2,1)}, u32[]{:S(2)}) copy-start(bf16[2,128,4,64]{1,3,2,0:T(8,128)(2,1)} %fusion.18) | copy-start | bytes 393220
  159.1 23.5 %collective-permute-start.8 = (bf16[288,2048]{1,0:T(8,128)(2,1)S(1)}, bf16[288,2048]{1,0:T(8,128)(2,1)S(1)}, u32[]{:S(2)}, u32[]{:S(2)}) collective-permute-start(bf16[288,2048]{1,0:T(8,128)(2,1)S(1)} %shard_map.174), channel_id=1, source_target_pairs={{0,6},{1,3},{2,0},{3,5},{4,2},{5,7},{6,4},{7,1},{8,14},{9,11},{10,... | collective-permute-start | bytes 3538952 | tf_op jit(solution)/shard_map/ppermute | solution.py:27
  170.1 5.6 %copy-start.10 = (bf16[1,896,2048]{2,1,0:T(8,128)(2,1)S(1)}, bf16[1,896,2048]{2,1,0:T(8,128)(2,1)}, u32[]{:S(2)}) copy-start(bf16[1,896,2048]{2,1,0:T(8,128)(2,1)} %param.31) | copy-start | bytes 11010052
  171.9 10.7 %collective-permute-start.14 = (bf16[288,2048]{1,0:T(8,128)(2,1)S(1)}, bf16[288,2048]{1,0:T(8,128)(2,1)S(1)}, u32[]{:S(2)}, u32[]{:S(2)}) collective-permute-start(bf16[288,2048]{1,0:T(8,128)(2,1)S(1)} %shard_map.179), channel_id=1, source_target_pairs={{0,1},{1,0},{2,3},{3,2},{4,5},{5,4},{6,7},{7,6},{8,9},{9,8},{10,11... | collective-permute-start | bytes 3538952 | tf_op jit(solution)/shard_map/ppermute | solution.py:32
  172.0 3.6 %copy-start.7 = (bf16[1,2048,896]{2,1,0:T(8,128)(2,1)S(1)}, bf16[1,2048,896]{2,1,0:T(8,128)(2,1)}, u32[]{:S(2)}) copy-start(bf16[1,2048,896]{2,1,0:T(8,128)(2,1)} %param.30) | copy-start | bytes 11010052
  172.8 2.2 %copy-start.16 = (f32[2,4,256,128,4]{3,2,4,1,0:T(8,128)}, f32[2,4,256,128,4]{3,2,4,1,0:T(8,128)S(1)}, u32[]{:S(2)}) copy-start(f32[2,4,256,128,4]{3,2,4,1,0:T(8,128)S(1)} %get-tuple-element.19) | copy-start | bytes 12582916
  172.9 2.0 copy-start.28
  172.9 3.8 %copy-start.4 = (bf16[1,2048,896]{2,1,0:T(8,128)(2,1)S(1)}, bf16[1,2048,896]{2,1,0:T(8,128)(2,1)}, u32[]{:S(2)}) copy-start(bf16[1,2048,896]{2,1,0:T(8,128)(2,1)} %param.29) | copy-start | bytes 11010052
  183.0 5.2 %copy-start.25 = (pred[2,128,256]{1,2,0:T(8,128)(4,1)S(1)}, pred[2,128,256]{1,2,0:T(8,128)(4,1)}, u32[]{:S(2)}) copy-start(pred[2,128,256]{1,2,0:T(8,128)(4,1)} %copy-done.24) | copy-start | bytes 196612
  183.1 5.2 %copy-start.27 = (bf16[2,128,4,64]{1,3,2,0:T(8,128)(2,1)S(1)}, bf16[2,128,4,64]{1,3,2,0:T(8,128)(2,1)}, u32[]{:S(2)}) copy-start(bf16[2,128,4,64]{1,3,2,0:T(8,128)(2,1)} %copy.36) | copy-start | bytes 393220
  183.1 5.2 %copy-start.29 = (f32[2,4,4,128]{3,2,1,0:T(4,128)S(1)}, f32[2,4,4,128]{3,2,1,0:T(4,128)}, u32[]{:S(2)}) copy-start(f32[2,4,4,128]{3,2,1,0:T(4,128)} %copy-done.28) | copy-start | bytes 49156
  183.1 5.2 %copy-start.30 = (f32[2,4,4,128]{3,2,1,0:T(4,128)S(1)}, f32[2,4,4,128]{3,2,1,0:T(4,128)}, u32[]{:S(2)}) copy-start(f32[2,4,4,128]{3,2,1,0:T(4,128)} %exponential_add_fusion) | copy-start | bytes 49156
  184.5 24.8 %all-to-all-start.1 = ((bf16[16,288,128]{2,1,0:T(8,128)(2,1)}), bf16[16,288,128]{2,1,0:T(8,128)(2,1)S(1)}, u32[]{:S(2)}, u32[]{:S(2)}) async-start(bf16[16,288,128]{2,1,0:T(8,128)(2,1)} %reshape.171), calls=%async_computation.1 | async-start | bytes 2359296 | tf_op jit(solution)/shard_map/all_to_all | solution.py:263
  188.3 4.1 %copy-start.36 = (bf16[1024,2048]{1,0:T(8,128)(2,1)S(1)}, bf16[1024,2048]{1,0:T(8,128)(2,1)}, u32[]{:S(2)}) copy-start(bf16[1024,2048]{1,0:T(8,128)(2,1)} %param.24) | copy-start | bytes 12582916
  192.3 18.8 %copy-start.1 = (bf16[2048,256]{1,0:T(8,128)(2,1)S(1)}, bf16[2048,256]{1,0:T(8,128)(2,1)}, u32[]{:S(2)}) copy-start(bf16[2048,256]{1,0:T(8,128)(2,1)} %param.19) | copy-start | bytes 3145732
  194.6 15.2 %copy-start.23 = (bf16[128,288]{0,1:T(8,128)(2,1)S(1)}, bf16[128,288]{0,1:T(8,128)(2,1)}, u32[]{:S(2)}) copy-start(bf16[128,288]{0,1:T(8,128)(2,1)} %fusion.19) | copy-start | bytes 221188

commit v2 on v1

--- a/solution.py
+++ b/solution.py
@@ -254,6 +254,42 @@
         out_specs=near,
         compiler_params=pltpu.CompilerParams(vmem_limit_bytes=12 << 20),
     )(*parts)
+
+
+def part_kernel(whole_ref, first_ref, second_ref):
+    count = first_ref.shape[0]
+    first_ref[...] = whole_ref[:count]
+    second_ref[...] = whole_ref[count:]
+
+
+def parted(whole):
+    near = pl.BlockSpec(memory_space=pltpu.VMEM)
+    return pl.pallas_call(
+        part_kernel,
+        out_shape=[jax.ShapeDtypeStruct((whole.shape[0] // 2, whole.shape[1]), whole.dtype)] * 2,
+        in_specs=[near],
+        out_specs=[near] * 2,
+        compiler_params=pltpu.CompilerParams(vmem_limit_bytes=12 << 20),
+    )(whole)
+
+
+def join_kernel(first_ref, second_ref, whole_ref):
+    count = first_ref.shape[0]
+    whole_ref[:count] = first_ref[...]
+    whole_ref[count:] = second_ref[...]
+
+
+def joined(first, second):
+    near = pl.BlockSpec(memory_space=pltpu.VMEM)
+    return pl.pallas_call(
+        join_kernel,
+        out_shape=jax.ShapeDtypeStruct(
+            (first.shape[0] + second.shape[0], first.shape[1]), first.dtype
+        ),
+        in_specs=[near] * 2,
+        out_specs=near,
+        compiler_params=pltpu.CompilerParams(vmem_limit_bytes=12 << 20),
+    )(first, second)
 
 
 def exchange(rows, experts):
@@ -303,10 +339,12 @@
     def run(blocks):
         return expert_partial(blocks, gate_weight[0], up_weight[0], down_weight[0])
 
-    near_a = outward(own, 1)
+    near_parts = [outward(part, 1) for part in parted(own)]
+    far_parts = [outward(part, 1) for part in near_parts]
+    near_a = joined(*near_parts)
+    far_a = joined(*far_parts)
     own_b = core_swap(own)
     near_b = outward(own_b, 1)
-    far_a = outward(near_a, 1)
     across_b = core_swap(near_a)
     across_a = core_swap(near_b)
     far_b = core_swap(far_a)
@@ -326,7 +364,8 @@
     passing = outward(far_sum, -1)
     home_a = outward(added(back_a, passing), -1)
     crossing = core_swap(added(own_part_b, home_b))
-    total = added(own_part_a, home_a, crossing)
+    settled = added(own_part_a, crossing)
+    total = added(settled, home_a)
     results = exchange(total, experts)
 
     gate_probs = jax.nn.softmax(route_logits, axis=-1).astype(jnp.bfloat16)

time: 212 us -> 209 us (0.986)
  the two profiles are of different devices: /device:TPU:1 before, /device:TPU:8 now
where the time goes in v2:
time: 209 us; the launch traced here: 205 us
  waiting for transfers between devices  64.5 us (31%)
  Pallas kernels  54.4 us (26%)
  local copies, waits for them, and re-layouts  35.8 us (17%)
  starting transfers between devices  27.1 us (13%)
  matrix products  13.2 us (6%)
  other arithmetic  8.91 us (4%)
    pallas_call x7, Pallas kernels, expert_partial(): pl.pallas_call(functools.partial(expert_kernel, count), out_shape=[jax.Sh...  43.2 us
    ppermute x8, waiting for transfers between devices, outward(): return lax.ppermute(block, 'tp', route)  33 us
    all_to_all x2, waiting for transfers between devices, exchange(): view = lax.all_to_all(view, 'ep', split_axis=0, concat_axis=0, tiled=True)  31.5 us
    unnamed x80, local copies, waits for them, and re-layouts  20.6 us
    all_to_all x2, starting transfers between devices, exchange(): view = lax.all_to_all(view, 'ep', split_axis=0, concat_axis=0, tiled=True)  11.7 us
    ppermute x8, starting transfers between devices, outward(): return lax.ppermute(block, 'tp', route)  10.7 us
    pallas_call x7, Pallas kernels, added(): pl.pallas_call(add_kernel, out_shape=jax.ShapeDtypeStruct(parts[0].shape,...  7.89 us
  transfers between devices with their start and end apart: 19, of which 8 were waited for; matrix products, arithmetic and copies ran while one was open for 16% of the time, Pallas kernels for 26%

profile of v2, /device:TPU:8, one launch (start us, length us, event | category | flops | bytes accessed | tf_op | source)
XLA Modules:
  0.0 205.1 jit_solution(10955548781307417704)
XLA Ops:
  0.7 1.1 copy-done.15
  1.8 0.7 copy-done.16
  3.2 0.8 shard_map.167
  4.0 1.4 reshape.169
  5.4 8.0 %all-to-all-start = ((bf16[16,288,128]{2,1,0:T(8,128)(2,1)}), bf16[16,288,128]{2,1,0:T(8,128)(2,1)S(1)}, u32[]{:S(2)}, u32[]{:S(2)}) async-start(bf16[16,288,128]{2,1,0:T(8,128)(2,1)} %reshape.169), calls=%async_computation | async-start | bytes 2359296 | tf_op jit(solution)/shard_map/all_to_all | solution.py:299
  13.7 18.9 %all-to-all-done = bf16[16,288,128]{2,1,0:T(8,128)(2,1)S(1)} async-done(((bf16[16,288,128]{2,1,0:T(8,128)(2,1)}), bf16[16,288,128]{2,1,0:T(8,128)(2,1)S(1)}, u32[]{:S(2)}, u32[]{:S(2)}) %all-to-all-start) | async-done | bytes 1179680 | tf_op jit(solution)/shard_map/all_to_all | solution.py:299
  33.4 2.0 multiply_reduce_fusion
  35.5 1.6 collective-permute-start.7
  37.2 1.3 collective-permute-start.8
  38.6 0.7 convolution_convert_fusion.2
  40.3 2.7 %collective-permute-start = (bf16[128,8,64]{0,2,1:T(8,128)(2,1)}, bf16[128,8,64]{0,2,1:T(8,128)(2,1)}, u32[]{:S(2)}, u32[]{:S(2)}) collective-permute-start(bf16[128,8,64]{0,2,1:T(8,128)(2,1)} %pad_maximum_fusion.2), channel_id=1, source_target_pairs={{0,1},{1,2},{2,3},{3,4},{4,5},{5,6},{6,7},{7,8},{8,9},{9,10},{10,1... | collective-permute-start | bytes 393224 | tf_op jit(solution)/shard_map/ppermute | solution.py:21
  43.0 2.6 %collective-permute-done.7.first_ref = bf16[144,2048]{1,0:T(8,128)(2,1)S(1)} collective-permute-done((bf16[144,2048]{1,0:T(8,128)(2,1)S(1)}, bf16[144,2048]{1,0:T(8,128)(2,1)S(1)}, u32[]{:S(2)}, u32[]{:S(2)}) %collective-permute-start.7) | collective-permute-done | bytes 589856 | tf_op jit(solution)/shard_map/ppermute | solution.py:27
  45.6 1.6 collective-permute-start.11
  47.1 6.1 %collective-permute-done.8.second_ref = bf16[144,2048]{1,0:T(8,128)(2,1)S(1)} collective-permute-done((bf16[144,2048]{1,0:T(8,128)(2,1)S(1)}, bf16[144,2048]{1,0:T(8,128)(2,1)S(1)}, u32[]{:S(2)}, u32[]{:S(2)}) %collective-permute-start.8) | collective-permute-done | bytes 589856 | tf_op jit(solution)/shard_map/ppermute | solution.py:27
  53.2 1.6 collective-permute-start.12
  54.8 2.7 %fusion.37 = (f32[256,1024]{1,0:T(8,128)}, f32[256,1024]{1,0:T(8,128)}) fusion(bf16[2048,1024]{1,0:T(8,128)(2,1)S(1)} %copy-done.35, bf16[256,2048]{1,0:T(8,128)(2,1)S(1)} %copy-done.21, f32[2048]{0:T(1024)S(1)} %copy-done.39, f32[256]{0:T(256)S(1)} %add_rsqrt_fusion.2), kind=kOutput, calls=%fused_computation.67 | convolution fusion | flops 1076101120 | bytes 7349248 | tf_op jit(solution)/shard_map/dot_general | solution.py:176
  57.4 2.6 %copy.40 = f32[256,1024]{0,1:T(8,128)} copy(f32[256,1024]{1,0:T(8,128)} %get-tuple-element.18) | data formatting | bytes 2097152 | tf_op jit(solution)/shard_map/mul | solution.py:38
  60.7 11.5 %collective-permute-done.11.first_ref = bf16[144,2048]{1,0:T(8,128)(2,1)S(1)} collective-permute-done((bf16[144,2048]{1,0:T(8,128)(2,1)S(1)}, bf16[144,2048]{1,0:T(8,128)(2,1)S(1)}, u32[]{:S(2)}, u32[]{:S(2)}) %collective-permute-start.11) | collective-permute-done | bytes 589856 | tf_op jit(solution)/shard_map/ppermute | solution.py:27
  72.2 0.8 copy-done.13
  73.0 5.6 %collective-permute-done.12.second_ref = bf16[144,2048]{1,0:T(8,128)(2,1)} collective-permute-done((bf16[144,2048]{1,0:T(8,128)(2,1)S(1)}, bf16[144,2048]{1,0:T(8,128)(2,1)}, u32[]{:S(2)}, u32[]{:S(2)}) %collective-permute-start.12) | collective-permute-done | bytes 589856 | tf_op jit(solution)/shard_map/ppermute | solution.py:27
  78.6 1.1 copy-done.14
  79.6 1.2 shard_map.179.refs_0_
  82.2 0.8 reshape.165
  83.7 1.7 fusion.18
  85.4 1.1 copy-done.12
  86.4 1.1 shard_map.176.refs_0_
  87.7 2.5 %copy.39 = f32[256,1024]{0,1:T(8,128)} copy(f32[256,1024]{1,0:T(8,128)} %get-tuple-element.19) | data formatting | bytes 2097152 | tf_op jit(solution)/shard_map/dot_general | solution.py:176
  90.2 1.7 reshape.166
  92.0 1.3 rsqrt.35
  93.3 2.2 %multiply_convert_fusion = bf16[2,128,4,4,64]{1,0,4,3,2:T(2,128)(2,1)} fusion(f32[2,128,4,4,64]{1,0,4,3,2:T(2,128)S(1)} %reshape.166, f32[64]{0:T(128)} %param.21, f32[2,128,4,4]{1,0,3,2:T(2,128)} %rsqrt.35), kind=kLoop, calls=%fused_computation.17 | loop fusion | flops 786432 | bytes 1589504 | tf_op jit(solution)/shard_map/convert_element_type | solution.py:177
  95.5 2.0 copy-done.2
  97.5 2.0 copy-done.5
  99.6 2.0 copy-done.8
  101.6 5.8 %shard_map.181 = bf16[288,2048]{1,0:T(8,128)(2,1)S(1)} custom-call(bf16[288,2048]{1,0:T(8,128)(2,1)} %collective-permute-done.13.refs_0_, bf16[2048,896]{1,0:T(8,128)(2,1)S(1)} %bitcast.73, bf16[2048,896]{1,0:T(8,128)(2,1)S(1)} %bitcast.80, bf16[896,2048]{1,0:T(8,128)(2,1)S(1)} %bitcast.87), custom_call_target="tpu_custom_call" | custom-call | flops 3170893824 | bytes 13369344 | tf_op jit(solution)/shard_map/pallas_call | solution.py:223
  108.1 5.8 %shard_map.171 = bf16[288,2048]{1,0:T(8,128)(2,1)S(1)} custom-call(bf16[288,2048]{1,0:T(8,128)(2,1)} %collective-permute-done.3.refs_0_, bf16[2048,896]{1,0:T(8,128)(2,1)S(1)} %bitcast.74, bf16[2048,896]{1,0:T(8,128)(2,1)S(1)} %bitcast.81, bf16[896,2048]{1,0:T(8,128)(2,1)S(1)} %bitcast.88), custom_call_target="tpu_custom_call" | custom-call | flops 3170893824 | bytes 13369344 | tf_op jit(solution)/shard_map/pallas_call | solution.py:223
  114.0 4.5 %shard_map.180.refs_0_ = bf16[288,2048]{1,0:T(8,128)(2,1)S(1)} custom-call(bf16[288,2048]{1,0:T(8,128)(2,1)S(1)} %shard_map.179.refs_0_, bf16[2048,896]{1,0:T(8,128)(2,1)S(1)} %bitcast.75, bf16[2048,896]{1,0:T(8,128)(2,1)S(1)} %bitcast.82, bf16[896,2048]{1,0:T(8,128)(2,1)S(1)} %bitcast.89), custom_call_target="tpu_custom_call" | custom-call | flops 3170893824 | bytes 13369344 | tf_op jit(solution)/shard_map/pallas_call | solution.py:223
  118.5 11.1 %shard_map.177 = (bf16[288,2048]{1,0:T(8,128)(2,1)S(1)}, bf16[288,2048]{1,0:T(8,128)(2,1)}) custom-call(bf16[288,2048]{1,0:T(8,128)(2,1)} %shard_map.176.refs_0_, bf16[288,2048]{1,0:T(8,128)(2,1)} %collective-permute-done.9.refs_1_, bf16[2048,896]{1,0:T(8,128)(2,1)S(1)} %bitcast.76, bf16[2048,896]{1,0:T(8,128)(2,1)S(1)} %bitcast.83, ...), custom_call_target="tpu_custom_call" | custom-call | flops 6341787648 | bytes 15728640 | tf_op jit(solution)/shard_map/pallas_call | solution.py:223
  130.1 5.8 %shard_map.170.refs_0_ = bf16[288,2048]{1,0:T(8,128)(2,1)S(1)} custom-call(bf16[288,2048]{1,0:T(8,128)(2,1)} %collective-permute-done.2.refs_0_, bf16[2048,896]{1,0:T(8,128)(2,1)S(1)} %bitcast.77, bf16[2048,896]{1,0:T(8,128)(2,1)S(1)} %bitcast.84, bf16[896,2048]{1,0:T(8,128)(2,1)S(1)} %bitcast.91), custom_call_target="tpu_custom_call" | custom-call | flops 3170893824 | bytes 13369344 | tf_op jit(solution)/shard_map/pallas_call | solution.py:223
  135.9 1.3 shard_map.182
  137.2 1.7 collective-permute-start.15
  138.9 1.3 shard_map.172
  140.2 1.8 collective-permute-start.5
  143.7 0.9 fusion.36
  144.7 2.0 copy-done.3
  146.7 2.0 copy-done.6
  148.7 2.0 copy-done.9
  150.8 5.8 %shard_map.169.refs_0_ = bf16[288,2048]{1,0:T(8,128)(2,1)S(1)} custom-call(bf16[288,2048]{1,0:T(8,128)(2,1)} %collective-permute-done.1.refs_0_, bf16[2048,896]{1,0:T(8,128)(2,1)S(1)} %bitcast.78, bf16[2048,896]{1,0:T(8,128)(2,1)S(1)} %bitcast.85, bf16[896,2048]{1,0:T(8,128)(2,1)S(1)} %bitcast.92), custom_call_target="tpu_custom_call" | custom-call | flops 3170893824 | bytes 13369344 | tf_op jit(solution)/shard_map/pallas_call | solution.py:223
  156.6 1.5 shard_map.178.refs_0_
  158.1 1.5 shard_map.183
  159.7 0.8 collective-permute-start.16
  160.5 5.9 %collective-permute-done.5.refs_1_ = bf16[288,2048]{1,0:T(8,128)(2,1)} collective-permute-done((bf16[288,2048]{1,0:T(8,128)(2,1)}, bf16[288,2048]{1,0:T(8,128)(2,1)}, u32[]{:S(2)}, u32[]{:S(2)}) %collective-permute-start.5) | collective-permute-done | bytes 1179680 | tf_op jit(solution)/shard_map/ppermute | solution.py:27
  166.4 1.7 shard_map.173
  168.2 0.8 fusion.1
  169.1 0.9 fusion
  170.1 1.1 copy-done.18
  171.3 1.6 copy-done.4
  172.9 4.5 %shard_map.168.refs_0_ = bf16[288,2048]{1,0:T(8,128)(2,1)S(1)} custom-call(bf16[288,2048]{1,0:T(8,128)(2,1)S(1)} %reshape.170.refs_0_.whole_ref, bf16[2048,896]{1,0:T(8,128)(2,1)S(1)} %bitcast.79, bf16[2048,896]{1,0:T(8,128)(2,1)S(1)} %bitcast.86, bf16[896,2048]{1,0:T(8,128)(2,1)S(1)} %bitcast.93), custom_call_target="tpu_custom_call" | custom-call | flops 3170893824 | bytes 13369344 | tf_op jit(solution)/shard_map/pallas_call | solution.py:223
  177.7 1.3 collective-permute-done.16.refs_1_
  179.2 1.4 reshape.171
  180.7 3.7 %all-to-all-start.1 = ((bf16[16,288,128]{2,1,0:T(8,128)(2,1)}), bf16[16,288,128]{2,1,0:T(8,128)(2,1)S(1)}, u32[]{:S(2)}, u32[]{:S(2)}) async-start(bf16[16,288,128]{2,1,0:T(8,128)(2,1)} %reshape.171), calls=%async_computation.1 | async-start | bytes 2359296 | tf_op jit(solution)/shard_map/all_to_all | solution.py:299
  184.4 3.5 %fusion.7 = bf16[2,128,4,4,64]{1,4,3,2,0:T(8,128)(2,1)S(1)} fusion(f32[2,4,256,128,4]{3,2,4,1,0:T(8,128)} %copy-done.18, f32[2,4,4,128]{3,2,1,0:T(4,128)S(1)} %exponential_add_fusion, f32[2,4,4,128]{3,2,1,0:T(4,128)S(1)} %broadcast_maximum_fusion, pred[2,128,256]{1,2,0:T(8,128)(4,1)S(1)} %broadcast_and_fusion, bf16[2,128,4,64]{1,3,2,0:T(8,128)(2,1)S(1)} %copy-done.30, ...), kind=kOutput, calls=%fused_computation.14 | convolution fusion | flops 140247040 | bytes 5079040 | tf_op jit(solution)/shard_map/bkgqs,bskd->bqkgd/dot_general | solution.py:143
  188.5 2.3 %convolution_convert_fusion = bf16[256,2048]{1,0:T(8,128)(2,1)} fusion(bf16[1024,2048]{1,0:T(8,128)(2,1)S(1)} %copy-done.36, bf16[128,8,2,128]{3,2,1,0:T(2,128)(2,1)S(1)} %bitcast.98), kind=kOutput, calls=%fused_computation.7 | convolution fusion | flops 1074266112 | bytes 5767168 | tf_op jit(solution)/shard_map/dot_general | solution.py:184
  190.7 12.6 %all-to-all-done.1 = bf16[16,288,128]{2,1,0:T(8,128)(2,1)S(1)} async-done(((bf16[16,288,128]{2,1,0:T(8,128)(2,1)}), bf16[16,288,128]{2,1,0:T(8,128)(2,1)S(1)}, u32[]{:S(2)}, u32[]{:S(2)}) %all-to-all-start.1) | async-done | bytes 1179680 | tf_op jit(solution)/shard_map/all_to_all | solution.py:299
  203.8 1.3 convolution_convert_fusion.1
  (119 shorter events, 10.5 us)
Async XLA Ops:
  0.6 32.7 %copy-start = (bf16[2048,256]{1,0:T(8,128)(2,1)S(1)}, bf16[2048,256]{1,0:T(8,128)(2,1)}, u32[]{:S(2)}) copy-start(bf16[2048,256]{1,0:T(8,128)(2,1)} %param.19) | copy-start | bytes 3145732
  0.6 1.1 copy-start.15
  1.8 0.7 copy-start.16
  2.5 0.7 copy-start.17
  5.4 8.0 %copy-start.20 = (bf16[256,2048]{1,0:T(8,128)(2,1)S(1)}, bf16[256,2048]{1,0:T(8,128)(2,1)}, u32[]{:S(2)}) copy-start(bf16[256,2048]{1,0:T(8,128)(2,1)} %param.16) | copy-start | bytes 3145732
  5.4 27.3 %all-to-all-start = ((bf16[16,288,128]{2,1,0:T(8,128)(2,1)}), bf16[16,288,128]{2,1,0:T(8,128)(2,1)S(1)}, u32[]{:S(2)}, u32[]{:S(2)}) async-start(bf16[16,288,128]{2,1,0:T(8,128)(2,1)} %reshape.169), calls=%async_computation | async-start | bytes 2359296 | tf_op jit(solution)/shard_map/all_to_all | solution.py:299
  13.4 19.9 %copy-start.38 = (f32[2048]{0:T(1024)S(1)}, f32[2048]{0:T(1024)}, u32[]{:S(2)}) copy-start(f32[2048]{0:T(1024)} %param.17) | copy-start | bytes 24580
  33.2 6.1 %collective-permute-start.1 = (bf16[288,2048]{1,0:T(8,128)(2,1)S(1)}, bf16[288,2048]{1,0:T(8,128)(2,1)}, u32[]{:S(2)}, u32[]{:S(2)}) collective-permute-start(bf16[288,2048]{1,0:T(8,128)(2,1)S(1)} %reshape.170.refs_0_.whole_ref), channel_id=1, source_target_pairs={{0,1},{1,0},{2,3},{3,2},{4,5},{5,4},{6,7},{7,6},{8,9},{9,8},{10,11... | collective-permute-start | bytes 3538952 | tf_op jit(solution)/shard_map/ppermute | solution.py:32
  33.3 5.1 %copy-start.32 = (f32[64]{0:T(128)S(1)}, f32[64]{0:T(128)}, u32[]{:S(2)}) copy-start(f32[64]{0:T(128)} %param.22) | copy-start | bytes 772
  33.3 5.2 %copy-start.21 = (bf16[256,2048]{1,0:T(8,128)(2,1)S(1)}, bf16[256,2048]{1,0:T(8,128)(2,1)}, u32[]{:S(2)}) copy-start(bf16[256,2048]{1,0:T(8,128)(2,1)} %param.16) | copy-start | bytes 3145732
  33.3 5.2 %copy-start.37 = (bf16[2048,256]{1,0:T(8,128)(2,1)S(1)}, bf16[2048,256]{1,0:T(8,128)(2,1)}, u32[]{:S(2)}) copy-start(bf16[2048,256]{1,0:T(8,128)(2,1)} %param.20) | copy-start | bytes 3145732
  33.3 5.2 %copy-start.39 = (f32[2048]{0:T(1024)S(1)}, f32[2048]{0:T(1024)}, u32[]{:S(2)}) copy-start(f32[2048]{0:T(1024)} %param.17) | copy-start | bytes 24580
  35.4 3.9 %copy-start.22 = (f32[256,256]{0,1:T(8,128)}, f32[256,256]{0,1:T(8,128)S(1)}, u32[]{:S(2)}) copy-start(f32[256,256]{0,1:T(8,128)S(1)} %get-tuple-element.21) | copy-start | bytes 786436
  35.4 19.4 %copy-start.35 = (bf16[2048,1024]{1,0:T(8,128)(2,1)S(1)}, bf16[2048,1024]{1,0:T(8,128)(2,1)}, u32[]{:S(2)}) copy-start(bf16[2048,1024]{1,0:T(8,128)(2,1)} %param.18) | copy-start | bytes 12582916
  35.5 10.0 %collective-permute-start.7 = (bf16[144,2048]{1,0:T(8,128)(2,1)S(1)}, bf16[144,2048]{1,0:T(8,128)(2,1)S(1)}, u32[]{:S(2)}, u32[]{:S(2)}) collective-permute-start(bf16[144,2048]{1,0:T(8,128)(2,1)S(1)} %get-tuple-element.10), channel_id=1, source_target_pairs={{0,2},{1,7},{2,4},{3,1},{4,6},{5,3},{6,0},{7,5},{8,10},{9,15},{10,... | collective-permute-start | bytes 1769480 | tf_op jit(solution)/shard_map/ppermute | solution.py:27
  37.2 16.0 %collective-permute-start.8 = (bf16[144,2048]{1,0:T(8,128)(2,1)S(1)}, bf16[144,2048]{1,0:T(8,128)(2,1)S(1)}, u32[]{:S(2)}, u32[]{:S(2)}) collective-permute-start(bf16[144,2048]{1,0:T(8,128)(2,1)S(1)} %get-tuple-element.11), channel_id=1, source_target_pairs={{0,2},{1,7},{2,4},{3,1},{4,6},{5,3},{6,0},{7,5},{8,10},{9,15},{10,... | collective-permute-start | bytes 1769480 | tf_op jit(solution)/shard_map/ppermute | solution.py:27
  39.3 18.1 %copy-start.24 = (bf16[256,256]{0,1:T(8,128)(2,1)}, bf16[256,256]{0,1:T(8,128)(2,1)S(1)}, u32[]{:S(2)}) copy-start(bf16[256,256]{0,1:T(8,128)(2,1)S(1)} %convolution_convert_fusion.2) | copy-start | bytes 393220
  39.3 42.4 %collective-permute-start.2 = (bf16[288,2048]{1,0:T(8,128)(2,1)}, bf16[288,2048]{1,0:T(8,128)(2,1)}, u32[]{:S(2)}, u32[]{:S(2)}) collective-permute-start(bf16[288,2048]{1,0:T(8,128)(2,1)} %collective-permute-done.1.refs_0_), channel_id=1, source_target_pairs={{0,2},{1,7},{2,4},{3,1},{4,6},{5,3},{6,0},{7,5},{8,10},{9,15},{10,... | collective-permute-start | bytes 3538952 | tf_op jit(solution)/shard_map/ppermute | solution.py:27
  40.3 103.4 %collective-permute-start = (bf16[128,8,64]{0,2,1:T(8,128)(2,1)}, bf16[128,8,64]{0,2,1:T(8,128)(2,1)}, u32[]{:S(2)}, u32[]{:S(2)}) collective-permute-start(bf16[128,8,64]{0,2,1:T(8,128)(2,1)} %pad_maximum_fusion.2), channel_id=1, source_target_pairs={{0,1},{1,2},{2,3},{3,4},{4,5},{5,6},{6,7},{7,8},{8,9},{9,10},{10,1... | collective-permute-start | bytes 393224 | tf_op jit(solution)/shard_map/ppermute | solution.py:21
  45.6 26.6 %collective-permute-start.11 = (bf16[144,2048]{1,0:T(8,128)(2,1)S(1)}, bf16[144,2048]{1,0:T(8,128)(2,1)S(1)}, u32[]{:S(2)}, u32[]{:S(2)}) collective-permute-start(bf16[144,2048]{1,0:T(8,128)(2,1)S(1)} %collective-permute-done.7.first_ref), channel_id=1, source_target_pairs={{0,2},{1,7},{2,4},{3,1},{4,6},{5,3},{6,0},{7,5},{8,10},{9,15},{10,... | collective-permute-start | bytes 1769480 | tf_op jit(solution)/shard_map/ppermute | solution.py:27
  53.2 4.2 %copy-start.11 = (bf16[144,2048]{1,0:T(8,128)(2,1)}, bf16[144,2048]{1,0:T(8,128)(2,1)S(1)}, u32[]{:S(2)}) copy-start(bf16[144,2048]{1,0:T(8,128)(2,1)S(1)} %collective-permute-done.8.second_ref) | copy-start | bytes 1769476
  53.2 25.4 %collective-permute-start.12 = (bf16[144,2048]{1,0:T(8,128)(2,1)S(1)}, bf16[144,2048]{1,0:T(8,128)(2,1)}, u32[]{:S(2)}, u32[]{:S(2)}) collective-permute-start(bf16[144,2048]{1,0:T(8,128)(2,1)S(1)} %collective-permute-done.8.second_ref), channel_id=1, source_target_pairs={{0,2},{1,7},{2,4},{3,1},{4,6},{5,3},{6,0},{7,5},{8,10},{9,15},{10,... | collective-permute-start | bytes 1769480 | tf_op jit(solution)/shard_map/ppermute | solution.py:27
  57.4 24.8 %copy-start.23 = (f32[256,256]{0,1:T(8,128)S(1)}, f32[256,256]{0,1:T(8,128)}, u32[]{:S(2)}) copy-start(f32[256,256]{0,1:T(8,128)} %copy-done.22) | copy-start | bytes 786436
  60.0 23.0 %copy-start.31 = (f32[128,2]{0,1:T(2,128)S(1)}, f32[128,2]{0,1:T(2,128)}, u32[]{:S(2)}) copy-start(f32[128,2]{0,1:T(2,128)} %param.28) | copy-start | bytes 3076
  72.2 0.8 copy-start.13
  78.6 1.1 copy-start.14
  79.6 1.4 copy-start.19
  80.9 14.6 %collective-permute-start.13 = (bf16[288,2048]{1,0:T(8,128)(2,1)S(1)}, bf16[288,2048]{1,0:T(8,128)(2,1)}, u32[]{:S(2)}, u32[]{:S(2)}) collective-permute-start(bf16[288,2048]{1,0:T(8,128)(2,1)S(1)} %shard_map.179.refs_0_), channel_id=1, source_target_pairs={{0,1},{1,0},{2,3},{3,2},{4,5},{5,4},{6,7},{7,6},{8,9},{9,8},{10,11... | collective-permute-start | bytes 3538952 | tf_op jit(solution)/shard_map/ppermute | solution.py:32
  81.8 26.3 %collective-permute-start.3 = (bf16[288,2048]{1,0:T(8,128)(2,1)}, bf16[288,2048]{1,0:T(8,128)(2,1)}, u32[]{:S(2)}, u32[]{:S(2)}) collective-permute-start(bf16[288,2048]{1,0:T(8,128)(2,1)} %collective-permute-done.2.refs_0_), channel_id=1, source_target_pairs={{0,1},{1,0},{2,3},{3,2},{4,5},{5,4},{6,7},{7,6},{8,9},{9,8},{10,11... | collective-permute-start | bytes 3538952 | tf_op jit(solution)/shard_map/ppermute | solution.py:32
  85.4 1.1 copy-start.12
  87.6 30.9 %collective-permute-start.9 = (bf16[288,2048]{1,0:T(8,128)(2,1)}, bf16[288,2048]{1,0:T(8,128)(2,1)}, u32[]{:S(2)}, u32[]{:S(2)}) collective-permute-start(bf16[288,2048]{1,0:T(8,128)(2,1)} %shard_map.176.refs_0_), channel_id=1, source_target_pairs={{0,1},{1,0},{2,3},{3,2},{4,5},{5,4},{6,7},{7,6},{8,9},{9,8},{10,11... | collective-permute-start | bytes 3538952 | tf_op jit(solution)/shard_map/ppermute | solution.py:32
  95.5 2.0 copy-start.2
  97.5 2.0 copy-start.5
  99.6 2.0 copy-start.8
  107.4 28.5 %collective-permute-start.14 = (bf16[288,2048]{1,0:T(8,128)(2,1)S(1)}, bf16[288,2048]{1,0:T(8,128)(2,1)S(1)}, u32[]{:S(2)}, u32[]{:S(2)}) collective-permute-start(bf16[288,2048]{1,0:T(8,128)(2,1)S(1)} %shard_map.181), channel_id=1, source_target_pairs={{0,1},{1,0},{2,3},{3,2},{4,5},{5,4},{6,7},{7,6},{8,9},{9,8},{10,11... | collective-permute-start | bytes 3538952 | tf_op jit(solution)/shard_map/ppermute | solution.py:32
  113.8 25.1 %collective-permute-start.4 = (bf16[288,2048]{1,0:T(8,128)(2,1)S(1)}, bf16[288,2048]{1,0:T(8,128)(2,1)S(1)}, u32[]{:S(2)}, u32[]{:S(2)}) collective-permute-start(bf16[288,2048]{1,0:T(8,128)(2,1)S(1)} %shard_map.171), channel_id=1, source_target_pairs={{0,1},{1,0},{2,3},{3,2},{4,5},{5,4},{6,7},{7,6},{8,9},{9,8},{10,11... | collective-permute-start | bytes 3538952 | tf_op jit(solution)/shard_map/ppermute | solution.py:32
  129.7 26.9 %collective-permute-start.10 = (bf16[288,2048]{1,0:T(8,128)(2,1)}, bf16[288,2048]{1,0:T(8,128)(2,1)}, u32[]{:S(2)}, u32[]{:S(2)}) collective-permute-start(bf16[288,2048]{1,0:T(8,128)(2,1)} %get-tuple-element.13), channel_id=1, source_target_pairs={{0,1},{1,0},{2,3},{3,2},{4,5},{5,4},{6,7},{7,6},{8,9},{9,8},{10,11... | collective-permute-start | bytes 3538952 | tf_op jit(solution)/shard_map/ppermute | solution.py:32
  137.2 4.8 %copy-start.28 = (pred[128,256]{0,1:T(8,128)(4,1)S(1)}, pred[128,256]{0,1:T(8,128)(4,1)}, u32[]{:S(2)}) copy-start(pred[128,256]{0,1:T(8,128)(4,1)} %fusion.24) | copy-start | bytes 98308
  137.2 4.8 %copy-start.33 = (pred[2,256]{1,0:T(4,128)(4,1)S(1)}, pred[2,256]{1,0:T(4,128)(4,1)}, u32[]{:S(2)}) copy-start(pred[2,256]{1,0:T(4,128)(4,1)} %add_compare_fusion) | copy-start | bytes 1540
  137.2 5.0 %copy-start.25 = (bf16[256,256]{0,1:T(8,128)(2,1)S(1)}, bf16[256,256]{0,1:T(8,128)(2,1)}, u32[]{:S(2)}) copy-start(bf16[256,256]{0,1:T(8,128)(2,1)} %copy-done.24) | copy-start | bytes 393220
  137.2 5.1 %copy-start.34 = (f32[16]{0:T(128)S(1)}, f32[16]{0:T(128)}, u32[]{:S(2)}) copy-start(f32[16]{0:T(128)} %param.23) | copy-start | bytes 196
  137.2 20.9 %collective-permute-start.15 = (bf16[288,2048]{1,0:T(8,128)(2,1)}, bf16[288,2048]{1,0:T(8,128)(2,1)}, u32[]{:S(2)}, u32[]{:S(2)}) collective-permute-start(bf16[288,2048]{1,0:T(8,128)(2,1)} %shard_map.182), channel_id=1, source_target_pairs={{0,6},{1,3},{2,0},{3,5},{4,2},{5,7},{6,4},{7,1},{8,14},{9,11},{10,... | collective-permute-start | bytes 3538952 | tf_op jit(solution)/shard_map/ppermute | solution.py:27
  140.2 26.2 %collective-permute-start.5 = (bf16[288,2048]{1,0:T(8,128)(2,1)}, bf16[288,2048]{1,0:T(8,128)(2,1)}, u32[]{:S(2)}, u32[]{:S(2)}) collective-permute-start(bf16[288,2048]{1,0:T(8,128)(2,1)} %shard_map.172), channel_id=1, source_target_pairs={{0,6},{1,3},{2,0},{3,5},{4,2},{5,7},{6,4},{7,1},{8,14},{9,11},{10,... | collective-permute-start | bytes 3538952 | tf_op jit(solution)/shard_map/ppermute | solution.py:27
  144.7 2.0 copy-start.3
  146.7 2.0 copy-start.6
  148.7 2.0 copy-start.9
  159.7 8.6 %copy-start.26 = (bf16[2,128,4,4,64]{1,0,4,3,2:T(2,128)(2,1)S(1)}, bf16[2,128,4,4,64]{1,0,4,3,2:T(2,128)(2,1)}, u32[]{:S(2)}) copy-start(bf16[2,128,4,4,64]{1,0,4,3,2:T(2,128)(2,1)} %multiply_convert_fusion) | copy-start | bytes 1572868
  159.7 8.6 %copy-start.29 = (bf16[2,128,4,64]{1,3,2,0:T(8,128)(2,1)S(1)}, bf16[2,128,4,64]{1,3,2,0:T(8,128)(2,1)}, u32[]{:S(2)}) copy-start(bf16[2,128,4,64]{1,3,2,0:T(8,128)(2,1)} %fusion.18) | copy-start | bytes 393220
  159.7 19.3 %collective-permute-start.16 = (bf16[288,2048]{1,0:T(8,128)(2,1)S(1)}, bf16[288,2048]{1,0:T(8,128)(2,1)S(1)}, u32[]{:S(2)}, u32[]{:S(2)}) collective-permute-start(bf16[288,2048]{1,0:T(8,128)(2,1)S(1)} %shard_map.183), channel_id=1, source_target_pairs={{0,6},{1,3},{2,0},{3,5},{4,2},{5,7},{6,4},{7,1},{8,14},{9,11},{10,... | collective-permute-start | bytes 3538952 | tf_op jit(solution)/shard_map/ppermute | solution.py:27
  166.4 4.8 %copy-start.10 = (bf16[1,896,2048]{2,1,0:T(8,128)(2,1)S(1)}, bf16[1,896,2048]{2,1,0:T(8,128)(2,1)}, u32[]{:S(2)}) copy-start(bf16[1,896,2048]{2,1,0:T(8,128)(2,1)} %param.31) | copy-start | bytes 11010052
  168.1 9.3 %collective-permute-start.6 = (bf16[288,2048]{1,0:T(8,128)(2,1)S(1)}, bf16[288,2048]{1,0:T(8,128)(2,1)S(1)}, u32[]{:S(2)}, u32[]{:S(2)}) collective-permute-start(bf16[288,2048]{1,0:T(8,128)(2,1)S(1)} %shard_map.173), channel_id=1, source_target_pairs={{0,1},{1,0},{2,3},{3,2},{4,5},{5,4},{6,7},{7,6},{8,9},{9,8},{10,11... | collective-permute-start | bytes 3538952 | tf_op jit(solution)/shard_map/ppermute | solution.py:32
  168.2 3.0 %copy-start.7 = (bf16[1,2048,896]{2,1,0:T(8,128)(2,1)S(1)}, bf16[1,2048,896]{2,1,0:T(8,128)(2,1)}, u32[]{:S(2)}) copy-start(bf16[1,2048,896]{2,1,0:T(8,128)(2,1)} %param.30) | copy-start | bytes 11010052
  169.0 2.1 %copy-start.18 = (f32[2,4,256,128,4]{3,2,4,1,0:T(8,128)}, f32[2,4,256,128,4]{3,2,4,1,0:T(8,128)S(1)}, u32[]{:S(2)}) copy-start(f32[2,4,256,128,4]{3,2,4,1,0:T(8,128)S(1)} %get-tuple-element.23) | copy-start | bytes 12582916
  169.1 3.7 %copy-start.4 = (bf16[1,2048,896]{2,1,0:T(8,128)(2,1)S(1)}, bf16[1,2048,896]{2,1,0:T(8,128)(2,1)}, u32[]{:S(2)}) copy-start(bf16[1,2048,896]{2,1,0:T(8,128)(2,1)} %param.29) | copy-start | bytes 11010052
  179.2 5.1 %copy-start.30 = (bf16[2,128,4,64]{1,3,2,0:T(8,128)(2,1)S(1)}, bf16[2,128,4,64]{1,3,2,0:T(8,128)(2,1)}, u32[]{:S(2)}) copy-start(bf16[2,128,4,64]{1,3,2,0:T(8,128)(2,1)} %copy.36) | copy-start | bytes 393220
  180.7 22.6 %all-to-all-start.1 = ((bf16[16,288,128]{2,1,0:T(8,128)(2,1)}), bf16[16,288,128]{2,1,0:T(8,128)(2,1)S(1)}, u32[]{:S(2)}, u32[]{:S(2)}) async-start(bf16[16,288,128]{2,1,0:T(8,128)(2,1)} %reshape.171), calls=%async_computation.1 | async-start | bytes 2359296 | tf_op jit(solution)/shard_map/all_to_all | solution.py:299
  184.4 4.1 %copy-start.36 = (bf16[1024,2048]{1,0:T(8,128)(2,1)S(1)}, bf16[1024,2048]{1,0:T(8,128)(2,1)}, u32[]{:S(2)}) copy-start(bf16[1024,2048]{1,0:T(8,128)(2,1)} %param.24) | copy-start | bytes 12582916
  188.5 16.7 %copy-start.1 = (bf16[2048,256]{1,0:T(8,128)(2,1)S(1)}, bf16[2048,256]{1,0:T(8,128)(2,1)}, u32[]{:S(2)}) copy-start(bf16[2048,256]{1,0:T(8,128)(2,1)} %param.19) | copy-start | bytes 3145732
  190.7 13.1 %copy-start.27 = (bf16[128,288]{0,1:T(8,128)(2,1)S(1)}, bf16[128,288]{0,1:T(8,128)(2,1)}, u32[]{:S(2)}) copy-start(bf16[128,288]{0,1:T(8,128)(2,1)} %fusion.19) | copy-start | bytes 221188
